TPU v7x, 256 devices: a whole 4x4x8 slice. The times are simulated.
256 devices in a mesh: dp: 4 (over x), kv: 32 (over z, y), tp: 2 (over core).
Axes of the slice: x: 4, y: 4, z: 8, core: 2. Of those that a mesh axis runs over, the one named last changes fastest.
Arguments:
- tokens: bfloat16 [4, 16384, 2048], P('dp', 'kv'), may hold values from -6 to 6
- w_query: bfloat16 [2048, 1024], P(None, 'tp'), as said below
- w_key: bfloat16 [2048, 1024], P(None, 'tp'), as said below
- w_value: bfloat16 [2048, 1024], P(None, 'tp'), may hold values from -0.125 to 0.125
- w_out: bfloat16 [1024, 2048], P('tp'), may hold values from -0.1875 to 0.1875
- chosen: int32 [4, 256, 16], P('dp', 'kv'), may hold values from -1 to 255, as said below
Outputs:
- mixed: bfloat16 [4, 16384, 2048], P('dp', ('kv', 'tp'))
- log_sums: float32 [4, 16, 16384], P('dp', 'tp', 'kv')
Inputs may be any that keep to these rules, and one draw needn't show every extreme that they name: `chosen`: write d = b // 8 and j = b % 8 for query block b. Row b lists b first, then min(15, j + 2 * d) distinct earlier blocks, then -1. Of the blocks that the query blocks of one index d of kv list, at most 2 lie in the positions of any one other index; the first query block of every index d >= 1 lists 2 blocks of index d - 1, and, where it exists, 2 blocks of the index half the sequence earlier. `w_query`: A weight matrix with entries up to about 4. `w_key`: A weight matrix of entries of order 2048 to the power -1/2.
All inputs are finite; a program needn't handle non-finite values.
Results may differ from a plain program's by a relative error of at most 0.0093.
Values may be sent and summed in bfloat16 or wider, within the bound.
A program may use at most 192 MiB of HBM per device.

v0:
```python
import jax
import jax.numpy as jnp
from jax import lax
from jax.sharding import PartitionSpec as P

HEAD_DIM = 64
BLOCK = 64


def in_blocks(shard, dim, devices):
    shape = shard.shape
    tiles = shard.reshape(*shape[:dim], devices, shape[dim] // devices, *shape[dim + 1 :])
    return jnp.moveaxis(tiles, dim, 0)


def summed_on_arrival(shard, axis, dim):
    devices = lax.axis_size(axis)
    tiles = lax.all_to_all(in_blocks(shard, dim, devices), axis, 0, 0, tiled=True)
    return jnp.sum(tiles.astype(jnp.float32), axis=0)


def on_device(tokens, w_query, w_key, w_value, w_out, chosen):
    inputs = tokens[0]
    listed = chosen[0]
    tok_rows = inputs.shape[0]
    queries = jnp.dot(inputs, w_query, preferred_element_type=jnp.float32).astype(jnp.bfloat16)
    keys_local = jnp.dot(inputs, w_key, preferred_element_type=jnp.float32).astype(jnp.bfloat16)
    values_local = jnp.dot(inputs, w_value, preferred_element_type=jnp.float32).astype(jnp.bfloat16)
    width = queries.shape[1]
    head_count = width // HEAD_DIM
    span_blocks = tok_rows // BLOCK
    query_count, picks = listed.shape
    myself = lax.axis_index("kv")
    valid = listed >= 0
    key_blocks = keys_local.reshape(span_blocks, BLOCK, width)
    value_blocks = values_local.reshape(span_blocks, BLOCK, width)
    kv_count = lax.axis_size("kv")
    capacity = max(1, min(2, span_blocks // 3))
    owners = jnp.where(valid, listed // span_blocks, myself)
    within = jnp.where(valid, listed % span_blocks, 0)
    foreign = valid & (owners != myself)
    owner_iota = jnp.arange(kv_count, dtype=jnp.int32)
    within_iota = jnp.arange(span_blocks, dtype=jnp.int32)
    hits = (
        (owners[:, :, None, None] == owner_iota[:, None])
        & (within[:, :, None, None] == within_iota[None, :])
        & foreign[:, :, None, None]
    )
    needed = jnp.any(hits, axis=(0, 1))
    order_rank = jnp.cumsum(needed.astype(jnp.int32), axis=1) - 1
    matches = needed[:, None, :] & (
        order_rank[:, None, :] == jnp.arange(capacity, dtype=jnp.int32)[None, :, None]
    )
    wanted = jnp.where(
        jnp.any(matches, axis=2), jnp.sum(matches.astype(jnp.int32) * within_iota, axis=2), -1
    )
    asked = lax.all_to_all(wanted, "kv", split_axis=0, concat_axis=0, tiled=True)
    present = (asked >= 0)[:, :, None, None]
    picked = jnp.clip(asked, 0, span_blocks - 1)
    zero_block = jnp.zeros((), jnp.bfloat16)
    send_keys = jnp.where(present, key_blocks[picked], zero_block)
    send_values = jnp.where(present, value_blocks[picked], zero_block)
    got_keys, got_values = (
        lax.all_to_all(send_keys, "kv", split_axis=0, concat_axis=0, tiled=True),
        lax.all_to_all(send_values, "kv", split_axis=0, concat_axis=0, tiled=True),
    )
    pool_keys = jnp.concatenate([key_blocks, got_keys.reshape(-1, BLOCK, width)], axis=0)
    pool_values = jnp.concatenate([value_blocks, got_values.reshape(-1, BLOCK, width)], axis=0)
    slot_rank = jnp.sum(hits.astype(jnp.int32) * order_rank[None, None], axis=(2, 3))
    slots = jnp.where(foreign, span_blocks + owners * capacity + slot_rank, within)
    keys_sel = pool_keys[slots].reshape(query_count, picks, BLOCK, head_count, HEAD_DIM)
    values_sel = pool_values[slots].reshape(query_count, picks, BLOCK, head_count, HEAD_DIM)
    query_blocks = queries.reshape(query_count, BLOCK, head_count, HEAD_DIM)
    scores = jnp.einsum(
        "nqhd,nskhd->nhqsk", query_blocks, keys_sel, preferred_element_type=jnp.float32
    ) * HEAD_DIM ** (-0.5)
    offsets = jnp.arange(BLOCK, dtype=jnp.int32)
    key_pos = listed[:, :, None] * BLOCK + offsets[None, None, :]
    query_pos = (myself * span_blocks + jnp.arange(query_count, dtype=jnp.int32))[
        :, None
    ] * BLOCK + offsets[None, :]
    allowed = valid[:, None, :, None] & (key_pos[:, None, :, :] <= query_pos[:, :, None, None])
    scores = jnp.where(allowed[:, None], scores, -jnp.inf)
    row_max = jnp.max(scores, axis=(3, 4), keepdims=True)
    exp_terms = jnp.exp(scores - row_max)
    row_sum = jnp.sum(exp_terms, axis=(3, 4), keepdims=True)
    weights = (exp_terms / row_sum).astype(jnp.bfloat16)
    attended = jnp.einsum(
        "nhqsk,nskhd->nqhd", weights, values_sel, preferred_element_type=jnp.float32
    )
    attended = attended.astype(jnp.bfloat16).reshape(tok_rows, width)
    log_sums = (row_max + jnp.log(row_sum))[:, :, :, 0, 0]
    log_sums = jnp.transpose(log_sums, (1, 0, 2)).reshape(head_count, tok_rows)
    mixed = summed_on_arrival(
        jnp.dot(attended, w_out, preferred_element_type=jnp.float32).astype(jnp.bfloat16), "tp", 0
    )
    return (mixed.astype(jnp.bfloat16)[None], log_sums[None])


def solution(mesh):
    return jax.shard_map(
        on_device,
        mesh=mesh,
        in_specs=(
            P("dp", "kv", None),
            P(None, "tp"),
            P(None, "tp"),
            P(None, "tp"),
            P("tp", None),
            P("dp", "kv", None),
        ),
        out_specs=(P("dp", ("kv", "tp"), None), P("dp", "tp", "kv")),
        check_vma=False,
    )
```

profile of v0, /device:TPU:1, one launch (start us, length us, event | category | flops | bytes accessed | tf_op | source)
XLA Modules:
  0.0 341.2 jit_solution(13670473937650168795)
XLA Ops:
  0.6 0.0 copy-start
  0.6 0.8 fusion.31
  1.5 0.1 iota_compare_fusion
  1.6 0.7 compare_and_fusion.1
  2.3 0.1 iota_compare_fusion.1
  2.4 0.3 fusion.27
  2.8 0.7 copy.43
  3.5 12.0 %all-to-all-start = ((s32[32,1,2]{2,1,0:T(1,128)}), s32[32,1,2]{2,1,0:T(1,128)S(1)}, u32[]{:S(2)}, u32[]{:S(2)}) async-start(s32[32,1,2]{2,1,0:T(1,128)} %copy.43), calls=%async_computation | async-start | bytes 32768 | tf_op jit(solution)/shard_map/all_to_all | solution.py:57
  15.6 0.0 copy-start.3
  15.6 0.0 copy-start.4
  15.6 3.6 %fusion.16 = bf16[512,512]{1,0:T(8,128)(2,1)S(1)} fusion(bf16[2048,512]{1,0:T(8,128)(2,1)} %param.9, bf16[1,512,2048]{2,1,0:T(8,128)(2,1)} %param.6), kind=kOutput, calls=%fused_computation.26 | convolution fusion | flops 1074003968 | bytes 4718592 | tf_op jit(solution)/shard_map/dot_general | solution.py:28
  19.2 1.2 fusion.22
  20.5 3.6 %all-to-all-done = s32[32,1,2]{2,1,0:T(1,128)S(1)} async-done(((s32[32,1,2]{2,1,0:T(1,128)}), s32[32,1,2]{2,1,0:T(1,128)S(1)}, u32[]{:S(2)}, u32[]{:S(2)}) %all-to-all-start) | async-done | bytes 288 | tf_op jit(solution)/shard_map/all_to_all | solution.py:57
  24.1 0.1 copy.44
  24.2 0.1 copy.47
  24.3 0.1 reshape.367
  24.4 0.1 copy.45
  24.5 2.7 gather_fusion
  27.2 2.8 gather_fusion.2
  30.0 5.1 %broadcast_select_fusion.1 = (bf16[32,2,64,512]{3,2,1,0:T(8,128)(2,1)}, bf16[32,2,64,512]{3,2,1,0:T(8,128)(2,1)S(1)}) fusion(bf16[32,2,64,512]{3,2,1,0:T(8,128)(2,1)} %bitcast.125, pred[32,2]{1,0:T(8,128)(4,1)S(1)} %copy.45, bf16[32,2,64,512]{3,2,1,0:T(8,128)(2,1)} %bitcast.126), kind=kLoop, calls=%fused_computation.16 | loop fusion | flops 4194304 | bytes 16777280 | tf_op jit(solution)/shard_map/jit(_where)/select_n | solution.py:62
  35.1 98.8 %all_to_all.21 = bf16[32,2,64,512]{3,2,1,0:T(8,128)(2,1)} all-to-all(bf16[32,2,64,512]{3,2,1,0:T(8,128)(2,1)S(1)} %get-tuple-element.7), channel_id=1, replica_groups=mesh['dp'=4,'kv'=32,'tp'=2] {'kv'}, dimensions={0} | all-to-all | bytes 8388608 | tf_op jit(solution)/shard_map/all_to_all | solution.py:64
  133.9 6.9 %all-to-all-start.1 = ((bf16[32,2,64,512]{3,2,1,0:T(8,128)(2,1)}), bf16[32,2,64,512]{3,2,1,0:T(8,128)(2,1)}, u32[]{:S(2)}, u32[]{:S(2)}) async-start(bf16[32,2,64,512]{3,2,1,0:T(8,128)(2,1)} %get-tuple-element.6), calls=%async_computation.1 | async-start | bytes 8388608 | tf_op jit(solution)/shard_map/all_to_all | solution.py:65
  140.9 2.6 select_reduce_fusion
  143.5 0.1 reshape.375
  143.6 4.3 %fusion.19 = bf16[512,512]{1,0:T(8,128)(2,1)} fusion(bf16[2048,512]{1,0:T(8,128)(2,1)} %param.7, bf16[1,512,2048]{2,1,0:T(8,128)(2,1)} %param.6), kind=kOutput, calls=%fused_computation.27 | convolution fusion | flops 1074003968 | bytes 4718592 | tf_op jit(solution)/shard_map/dot_general | solution.py:26
  147.9 2.4 reshape.359
  150.3 0.1 iota_add_fusion.1
  150.4 0.1 iota_add_fusion
  150.4 2.6 compare_and_fusion
  153.0 4.7 %pad_maximum_fusion.1 = bf16[72,64,512]{2,1,0:T(8,128)(2,1)} fusion(bf16[64,64,512]{2,1,0:T(8,128)(2,1)} %bitcast.127, bf16[8,64,512]{2,1,0:T(8,128)(2,1)S(1)} %bitcast.124), kind=kLoop, calls=%fused_computation.13 | loop fusion | flops 2359296 | bytes 9437184 | tf_op jit(solution)/shard_map/concatenate | solution.py:67
  157.7 8.7 %gather_fusion.3 = bf16[128,64,512]{2,1,0:T(8,128)(2,1)} fusion(bf16[72,64,512]{2,1,0:T(8,128)(2,1)} %pad_maximum_fusion.1, s32[1024]{0:T(1024)S(1)} %pad_clamp_fusion), kind=kCustom, calls=%fused_computation.3 | custom fusion | bytes 16777728 | tf_op jit(solution)/shard_map/gather | solution.py:71
  166.4 21.2 %reshape.362 = bf16[8,16,64,8,64]{4,3,2,1,0:T(8,128)(2,1)} reshape(bf16[128,64,512]{2,1,0:T(8,128)(2,1)} %gather_fusion.3) | data formatting | bytes 16777216 | tf_op jit(solution)/shard_map/reshape | solution.py:71
  187.6 15.1 %copy.49 = bf16[8,16,64,8,64]{4,2,1,3,0:T(8,128)(2,1)} copy(bf16[8,16,64,8,64]{4,3,2,1,0:T(8,128)(2,1)} %reshape.362) | data formatting | bytes 16777216 | tf_op jit(solution)/shard_map/reshape | solution.py:71
  202.8 30.8 %all-to-all-done.1 = bf16[32,2,64,512]{3,2,1,0:T(8,128)(2,1)} async-done(((bf16[32,2,64,512]{3,2,1,0:T(8,128)(2,1)}), bf16[32,2,64,512]{3,2,1,0:T(8,128)(2,1)}, u32[]{:S(2)}, u32[]{:S(2)}) %all-to-all-start.1) | async-done | bytes 4194336 | tf_op jit(solution)/shard_map/all_to_all | solution.py:65
  233.6 4.7 %pad_maximum_fusion = bf16[72,64,512]{2,1,0:T(8,128)(2,1)} fusion(bf16[64,64,512]{2,1,0:T(8,128)(2,1)} %bitcast.7, bf16[8,64,512]{2,1,0:T(8,128)(2,1)S(1)} %bitcast.122), kind=kLoop, calls=%fused_computation.12 | loop fusion | flops 2359296 | bytes 9437184 | tf_op jit(solution)/shard_map/concatenate | solution.py:68
  238.3 8.7 %gather_fusion.1 = bf16[128,64,512]{2,1,0:T(8,128)(2,1)} fusion(bf16[72,64,512]{2,1,0:T(8,128)(2,1)} %pad_maximum_fusion, s32[1024]{0:T(1024)S(1)} %pad_clamp_fusion), kind=kCustom, calls=%fused_computation.1 | custom fusion | bytes 16777728 | tf_op jit(solution)/shard_map/gather | solution.py:72
  247.0 21.3 %reshape.358 = bf16[8,16,64,8,64]{4,3,2,1,0:T(8,128)(2,1)} reshape(bf16[128,64,512]{2,1,0:T(8,128)(2,1)} %gather_fusion.1) | data formatting | bytes 16777216 | tf_op jit(solution)/shard_map/reshape | solution.py:72
  268.3 17.8 %fusion = (f32[8,8,64]{2,1,0:T(8,128)S(1)}, f32[8,8,64,1024]{2,3,1,0}) fusion(pred[8,64,16,64]{1,3,2,0:T(8,128)(4,1)S(1)} %copy-done.1, bf16[8,8,64,1024]{2,3,1,0:T(8,128)(2,1)} %bitcast.120, bf16[8,64,8,64]{3,2,1,0:T(8,128)(2,1)} %reshape.359), kind=kOutput, calls=%fused_computation.7 | convolution fusion | flops 549449728 | bytes 26230784
  286.1 14.7 %fusion.1 = f32[8,8,64]{2,1,0:T(8,128)S(1)} fusion(f32[8,8,64,1024]{2,3,1,0} %get-tuple-element.10, f32[8,8,64]{2,1,0:T(8,128)S(1)} %get-tuple-element.9, pred[8,64,16,64]{1,3,2,0:T(8,128)(4,1)S(1)} %copy-done.1), kind=kLoop, calls=%fused_computation.8 | loop fusion | flops 16773120 | bytes 17334272 | tf_op jit(solution)/shard_map/reduce_sum | solution.py:86
  300.8 20.5 %fusion.13 = bf16[8,64,8,64]{1,3,2,0:T(8,128)(2,1)} fusion(f32[8,8,64,1024]{2,3,1,0} %get-tuple-element.10, f32[8,8,64]{2,1,0:T(8,128)S(1)} %fusion.1, f32[8,8,64]{2,1,0:T(8,128)S(1)} %get-tuple-element.9, pred[8,64,16,64]{1,3,2,0:T(8,128)(4,1)S(1)} %copy-done.1, bf16[8,16,64,8,64]{4,3,2,1,0:T(8,128)(2,1)} %reshape.358), kind=kOutput, calls=%fused_computation.25 | convolution fusion | flops 558104576 | bytes 26247168 | tf_op jit(solution)/shard_map/nhqsk,nskhd->nqhd/dot_general | solution.py:88
  321.3 1.7 copy.52
  323.0 1.4 reshape.363
  324.4 0.0 copy-done
  324.4 3.6 %convolution_convert_fusion = bf16[512,2048]{1,0:T(8,128)(2,1)} fusion(bf16[512,512]{1,0:T(8,128)(2,1)} %reshape.363, bf16[512,2048]{1,0:T(8,128)(2,1)S(1)} %copy-done), kind=kOutput, calls=%fused_computation.17 | convolution fusion | flops 1074790400 | bytes 4718592 | tf_op jit(solution)/shard_map/dot_general | solution.py:95
  328.0 7.3 %all-to-all-start.3 = ((bf16[2,256,2048]{2,1,0:T(8,128)(2,1)}), bf16[2,256,2048]{2,1,0:T(8,128)(2,1)}, u32[]{:S(2)}, u32[]{:S(2)}) async-start(bf16[2,256,2048]{2,1,0:T(8,128)(2,1)} %bitcast.128), calls=%async_computation.3 | async-start | bytes 4194304 | tf_op jit(solution)/shard_map/all_to_all | solution.py:18
  335.2 0.7 broadcast_in_dim_reshape.3
  335.9 1.9 all-to-all-done.3
  337.9 3.3 reduce_sum.45
  (20 shorter events, 0.2 us)
Async XLA Ops:
  0.6 323.8 %copy-start = (bf16[512,2048]{1,0:T(8,128)(2,1)S(1)}, bf16[512,2048]{1,0:T(8,128)(2,1)}, u32[]{:S(2)}) copy-start(bf16[512,2048]{1,0:T(8,128)(2,1)} %param.10) | copy-start | bytes 6291460
  3.5 20.6 %all-to-all-start = ((s32[32,1,2]{2,1,0:T(1,128)}), s32[32,1,2]{2,1,0:T(1,128)S(1)}, u32[]{:S(2)}, u32[]{:S(2)}) async-start(s32[32,1,2]{2,1,0:T(1,128)} %copy.43), calls=%async_computation | async-start | bytes 32768 | tf_op jit(solution)/shard_map/all_to_all | solution.py:57
  15.6 3.6 %copy-start.3 = (bf16[2048,512]{1,0:T(8,128)(2,1)S(1)}, bf16[2048,512]{1,0:T(8,128)(2,1)}, u32[]{:S(2)}) copy-start(bf16[2048,512]{1,0:T(8,128)(2,1)} %param.8) | copy-start | bytes 6291460
  15.6 3.6 %copy-start.4 = (bf16[1,512,2048]{2,1,0:T(8,128)(2,1)S(1)}, bf16[1,512,2048]{2,1,0:T(8,128)(2,1)}, u32[]{:S(2)}) copy-start(bf16[1,512,2048]{2,1,0:T(8,128)(2,1)} %param.6) | copy-start | bytes 6291460
  133.9 9.6 %copy-start.2 = (s32[1,8,16]{2,1,0:T(8,128)S(1)}, s32[1,8,16]{2,1,0:T(8,128)}, u32[]{:S(2)}) copy-start(s32[1,8,16]{2,1,0:T(8,128)} %param.11) | copy-start | bytes 1540
  133.9 99.6 %all-to-all-start.1 = ((bf16[32,2,64,512]{3,2,1,0:T(8,128)(2,1)}), bf16[32,2,64,512]{3,2,1,0:T(8,128)(2,1)}, u32[]{:S(2)}, u32[]{:S(2)}) async-start(bf16[32,2,64,512]{3,2,1,0:T(8,128)(2,1)} %get-tuple-element.6), calls=%async_computation.1 | async-start | bytes 8388608 | tf_op jit(solution)/shard_map/all_to_all | solution.py:65
  247.0 21.3 %copy-start.1 = (pred[8,64,16,64]{1,3,2,0:T(8,128)(4,1)S(1)}, pred[8,64,16,64]{1,3,2,0:T(8,128)(4,1)}, u32[]{:S(2)}) copy-start(pred[8,64,16,64]{1,3,2,0:T(8,128)(4,1)} %compare_and_fusion) | copy-start | bytes 1572868
  328.0 9.9 %all-to-all-start.3 = ((bf16[2,256,2048]{2,1,0:T(8,128)(2,1)}), bf16[2,256,2048]{2,1,0:T(8,128)(2,1)}, u32[]{:S(2)}, u32[]{:S(2)}) async-start(bf16[2,256,2048]{2,1,0:T(8,128)(2,1)} %bitcast.128), calls=%async_computation.3 | async-start | bytes 4194304 | tf_op jit(solution)/shard_map/all_to_all | solution.py:18
where the time goes:
time: 344 us; the launch traced here: 341 us
  blocking collectives  98.8 us (29%)
  local copies, waits for them, and re-layouts  87.9 us (26%)
  matrix products  51 us (15%)
  other arithmetic  40.1 us (12%)
  waiting for transfers between devices  36.4 us (11%)
  starting transfers between devices  26.2 us (8%)
    all_to_all x1, blocking collectives, on_device(): lax.all_to_all(send_keys, 'kv', split_axis=0, concat_axis=0, tiled=True)  98.8 us
    reshape x2, local copies, waits for them, and re-layouts, on_device(): pool_keys[slots].reshape(query_count, picks, BLOCK, head_count, HEAD_DIM)  36.4 us
    all_to_all x1, waiting for transfers between devices, on_device(): lax.all_to_all(send_values, 'kv', split_axis=0, concat_axis=0, tiled=True)  30.8 us
    reshape x1, local copies, waits for them, and re-layouts, on_device(): pool_values[slots].reshape(query_count, picks, BLOCK, head_count, HEAD_DIM)  21.3 us
    dot_general x1, matrix products, on_device(): jnp.einsum('nhqsk,nskhd->nqhd', weights, values_sel, preferred_element_ty...  20.5 us
    unnamed x1, matrix products  17.8 us
    reduce_sum x1, other arithmetic, on_device(): row_sum = jnp.sum(exp_terms, axis=(3, 4), keepdims=True)  14.7 us
    all_to_all x1, starting transfers between devices, on_device(): lax.all_to_all(wanted, 'kv', split_axis=0, concat_axis=0, tiled=True)  12 us
  transfers between devices with their start and end apart: 3, of which 3 were waited for; matrix products, arithmetic and copies ran while one was open for 20% of the time, Pallas kernels for 0%

commit v1 on v0

v1 whole, which is shorter than its diff:
```python
import functools

import jax
import jax.numpy as jnp
from jax import lax
from jax.experimental import pallas as pl
from jax.experimental.pallas import tpu as pltpu
from jax.sharding import PartitionSpec as P

HEAD_DIM = 64
BLOCK = 64
NZ = 8
NY = 4
PICKS = 16
LOG2E = 1.4426950408889634
MESH = pl.DeviceIdType.MESH
BF16 = jnp.bfloat16
F32 = jnp.float32


def order(step, me_z):
    half = (step + 1) // 2
    return lax.rem(me_z + jnp.where(lax.rem(step, 2) == 1, half, NZ - half), NZ)


def kernel(
    x_hbm, wq_hbm, wk_hbm, wv_hbm, wo_hbm, chosen_ref, out_ref, logs_ref,
    x, wkv, wq, wo, kvs, land, qs, qland, cs, cland, picks, gathered, os, oland, stat, ls, lland, att,
    in_sem, wo_sem, wo_send, wo_recv, own_sem, own_out_sem, pick_sem,
    kv_send, kv_recv, q_send, q_recv, c_send, c_recv,
    y_send, y_recv, f_send, f_recv, o_send, o_recv, l_send, l_recv,
):
    kv = lax.axis_index("kv")
    core = lax.axis_index("tp")
    me_z, me_y = kv // NY, lax.rem(kv, NY)
    rows = x.shape[0]
    half = rows // 2
    blocks = rows // BLOCK
    up = me_z * NY + lax.rem(me_y + 1, NY)
    down = me_z * NY + lax.rem(me_y + NY - 1, NY)
    below = lax.rem(me_y + NY - 1, NY)
    above = lax.rem(me_y + 1, NY)

    def at(z):
        return z * NY + me_y

    x_copy = pltpu.make_async_copy(x_hbm, x, in_sem.at[0])
    x_copy.start()
    w_copies = []
    for p in range(4):
        pair = []
        for i, src in enumerate((wk_hbm, wv_hbm)):
            c = pltpu.make_async_copy(
                src.at[:, pl.ds(p * 128, 128)], wkv.at[p, :, pl.ds(i * 128, 128)], in_sem.at[1 + 2 * p + i]
            )
            c.start()
            pair.append(c)
        w_copies.append(pair)
    wq_copy = pltpu.make_async_copy(wq_hbm, wq, in_sem.at[9])
    wq_copy.start()

    barrier = pltpu.get_barrier_semaphore()
    for k in range(NZ):
        z = lax.rem(me_z + k, NZ)
        for c in range(2):
            if k == 0 and c == 0:
                pl.semaphore_signal(barrier, inc=1, device_id={"tp": 1 - core}, device_id_type=MESH)
            elif k > 0:
                pl.semaphore_signal(barrier, inc=1, device_id={"kv": at(z), "tp": c}, device_id_type=MESH)
    for peer in (up, down):
        pl.semaphore_signal(barrier, inc=1, device_id={"kv": peer}, device_id_type=MESH)

    cs[...] = jnp.zeros_like(cs)
    cs[:, 0:PICKS] = jnp.maximum(chosen_ref[...], 0)
    lane = lax.broadcasted_iota(jnp.int32, (rows, 128), 1)
    low = lane < HEAD_DIM

    x_copy.wait()
    for p in range(4):
        for c in w_copies[p]:
            c.wait()

    def project_pair(p, carry):
        both = jnp.dot(x[...], wkv[p], preferred_element_type=F32)
        kp, vp = both[:, 0:128], both[:, 128:256]
        kvs[2 * p] = jnp.where(low, kp, pltpu.roll(vp, HEAD_DIM, 1)).astype(BF16).reshape(blocks, BLOCK, 128)
        kvs[2 * p + 1] = jnp.where(low, pltpu.roll(kp, HEAD_DIM, 1), vp).astype(BF16).reshape(blocks, BLOCK, 128)
        return carry

    lax.fori_loop(0, 4, project_pair, 0)
    pl.semaphore_wait(barrier, 2 * NZ + 1)

    def kv_copy(z):
        return pltpu.make_async_remote_copy(
            src_ref=kvs.at[z], dst_ref=land.at[pl.ds(kv * blocks, blocks)], send_sem=kv_send.at[z],
            recv_sem=kv_recv.at[me_z], device_id={"kv": at(z)}, device_id_type=MESH,
        )

    def kv_arrival(z):
        return pltpu.make_async_remote_copy(
            src_ref=kvs.at[z], dst_ref=land.at[pl.ds(at(z) * blocks, blocks)], send_sem=kv_send.at[z],
            recv_sem=kv_recv.at[z], device_id={"kv": at(z)}, device_id_type=MESH,
        )

    def q_copy(z, src):
        return pltpu.make_async_remote_copy(
            src_ref=qs.at[z], dst_ref=qland.at[src], send_sem=q_send.at[z],
            recv_sem=q_recv.at[src], device_id={"kv": at(z)}, device_id_type=MESH,
        )

    def c_copy(z, src):
        return pltpu.make_async_remote_copy(
            src_ref=cs, dst_ref=cland.at[src], send_sem=c_send.at[z],
            recv_sem=c_recv.at[src], device_id={"kv": at(z)}, device_id_type=MESH,
        )

    own_kv = pltpu.make_async_copy(kvs.at[me_z], land.at[pl.ds(kv * blocks, blocks)], own_sem.at[0])
    own_kv.start()
    own_c = pltpu.make_async_copy(cs, cland.at[me_z], own_sem.at[1])
    own_c.start()
    for t in range(1, NZ):
        c_copy(order(t, me_z), me_z).start()
    for t in range(1, NZ):
        kv_copy(order(t, me_z)).start()

    wo_rows = wo_hbm.shape[0]
    wo_mine = wo.at[pl.ds(core * wo_rows, wo_rows)]
    wo_local = pltpu.make_async_copy(wo_hbm, wo_mine, wo_sem)
    wo_local.start()
    wo_remote = pltpu.make_async_remote_copy(
        src_ref=wo_hbm, dst_ref=wo_mine, send_sem=wo_send, recv_sem=wo_recv,
        device_id={"tp": 1 - core}, device_id_type=MESH,
    )
    wo_remote.start()

    wq_copy.wait()

    def project_queries(i, carry):
        res = jnp.dot(x[...], wq[:, pl.ds(pl.multiple_of(i * 256, 256), 256)], preferred_element_type=F32)
        lo = low[:half]
        for u in range(2):
            top, bot = res[:half, u * 128:(u + 1) * 128], res[half:, u * 128:(u + 1) * 128]
            qs[4 * i + 2 * u] = jnp.where(lo, top, pltpu.roll(bot, HEAD_DIM, 1)).astype(BF16)
            qs[4 * i + 2 * u + 1] = jnp.where(lo, pltpu.roll(top, HEAD_DIM, 1), bot).astype(BF16)
        return carry

    lax.fori_loop(0, 2, project_queries, 0)
    own_q = pltpu.make_async_copy(qs.at[me_z], qland.at[me_z], own_sem.at[2])
    own_q.start()
    for t in range(1, NZ):
        q_copy(order(t, me_z), me_z).start()

    def y_copy(z, way):
        rng = pl.ds(at(z) * blocks, blocks)
        return pltpu.make_async_remote_copy(
            src_ref=land.at[rng], dst_ref=land.at[rng], send_sem=y_send.at[z, way],
            recv_sem=y_recv.at[z, way], device_id={"kv": (up, down)[way]}, device_id_type=MESH,
        )

    def y_arrival(z, way):
        rng = pl.ds((z * NY + (below, above)[way]) * blocks, blocks)
        return pltpu.make_async_remote_copy(
            src_ref=land.at[rng], dst_ref=land.at[rng], send_sem=y_send.at[z, way],
            recv_sem=y_recv.at[z, way], device_id={"kv": (up, down)[way]}, device_id_type=MESH,
        )

    def f_copy(z, way):
        rng = pl.ds((z * NY + (below, above)[way]) * blocks + way * (blocks // 2), blocks // 2)
        return pltpu.make_async_remote_copy(
            src_ref=land.at[rng], dst_ref=land.at[rng], send_sem=f_send.at[z, way],
            recv_sem=f_recv.at[z, way], device_id={"kv": (up, down)[way]}, device_id_type=MESH,
        )

    far = lax.rem(me_y + 2, NY)

    def f_arrival(z, way):
        rng = pl.ds((z * NY + far) * blocks + way * (blocks // 2), blocks // 2)
        return pltpu.make_async_remote_copy(
            src_ref=land.at[rng], dst_ref=land.at[rng], send_sem=f_send.at[z, way],
            recv_sem=f_recv.at[z, way], device_id={"kv": (up, down)[way]}, device_id_type=MESH,
        )

    own_kv.wait()
    for t in range(NZ + 1):
        if t < NZ:
            z = order(t, me_z)
            if t > 0:
                kv_arrival(z).wait_recv()
            for way in range(2):
                y_copy(z, way).start()
        if t > 0:
            z = order(t - 1, me_z)
            for way in range(2):
                y_arrival(z, way).wait_recv()
                f_copy(z, way).start()
    for z in range(NZ):
        for way in range(2):
            f_arrival(z, way).wait_recv()

    own_c.wait()
    own_q.wait()
    for t in range(1, NZ):
        z = order(t, me_z)
        c_copy(z, z).wait_recv()
    to_scalars = pltpu.make_async_copy(cland, picks, pick_sem)
    to_scalars.start()
    to_scalars.wait()

    row_iota = lax.broadcasted_iota(jnp.int32, (128, 128), 0)
    lane_iota = lax.broadcasted_iota(jnp.int32, (128, 128), 1)
    low64 = lax.broadcasted_iota(jnp.int32, (BLOCK, 128), 1) < HEAD_DIM
    key_iota = lax.broadcasted_iota(jnp.int32, (128, PICKS * BLOCK), 1)
    row_col = lax.broadcasted_iota(jnp.int32, (128, 1), 0)
    hidden = (lane_iota < BLOCK) & (lane_iota > lax.rem(row_iota, BLOCK))
    zero = jnp.zeros((BLOCK, 128), BF16)

    def o_copy(g, to):
        return pltpu.make_async_remote_copy(
            src_ref=os.at[g, to], dst_ref=oland.at[core * NZ + me_z], send_sem=o_send.at[g, to],
            recv_sem=o_recv.at[core * NZ + me_z], device_id={"kv": at(g), "tp": to}, device_id_type=MESH,
        )

    def l_copy(g, src):
        return pltpu.make_async_remote_copy(
            src_ref=ls.at[g], dst_ref=lland.at[src], send_sem=l_send.at[g],
            recv_sem=l_recv.at[src], device_id={"kv": at(g)}, device_id_type=MESH,
        )

    def attend_group(t, carry):
        g = order(t, me_z)

        @pl.when(t > 0)
        def _():
            q_copy(g, g).wait_recv()

        def attend_pair(j, carry):
            for s in range(PICKS):
                for i in range(2):
                    gathered[pl.ds(s * BLOCK, BLOCK), pl.ds(i * 128, 128)] = land[picks[g, j + 4 * i, s]]
            tile = qland[g, pl.ds(pl.multiple_of(j * BLOCK, BLOCK), BLOCK), :].astype(F32)
            first = jnp.where(low64, tile, 0.0).astype(BF16)
            second = jnp.where(low64, pltpu.roll(tile, HEAD_DIM, 1), 0.0).astype(BF16)
            lhs = jnp.concatenate(
                [jnp.concatenate([first, zero], axis=1), jnp.concatenate([zero, second], axis=1)], axis=0
            )
            s = lax.dot_general(lhs, gathered[...], (((1,), (1,)), ((), ())), preferred_element_type=F32)
            device = g * NY + me_y
            limit = (jnp.where(row_col < BLOCK, j, j + 4) + 2 * device + 1) * BLOCK
            s = jnp.where(key_iota < limit, s, -jnp.inf)
            s = jnp.concatenate([jnp.where(hidden, -jnp.inf, s[:, 0:128]), s[:, 128:]], axis=1)
            peak = jnp.max(s, axis=1, keepdims=True)
            e = jnp.exp2((s - peak) * (LOG2E * HEAD_DIM ** -0.5))
            total = jnp.sum(e, axis=1, keepdims=True)
            o = jnp.dot(e.astype(BF16), gathered[...], preferred_element_type=F32) * (1.0 / total)
            log_sum = peak * HEAD_DIM ** -0.5 + jnp.log(total)
            stat[...] = jnp.where(lane_iota == j, log_sum, stat[...])
            place = pl.ds(pl.multiple_of(lax.rem(j, 2) * BLOCK, BLOCK), BLOCK)
            for i in range(2):
                part = o[i * BLOCK:(i + 1) * BLOCK, i * 128:(i + 1) * 128]
                old = os[g, i, place, :].astype(F32)
                left = jnp.where(j < 2, pltpu.roll(part, HEAD_DIM, 1), old)
                os[g, i, place, :] = jnp.where(low64, left, part).astype(BF16)
            return carry

        lax.fori_loop(0, 4, attend_pair, 0)
        ls[g] = stat[...].T[0:8]

        @pl.when(g != me_z)
        def _():
            o_copy(g, 0).start()
            o_copy(g, 1).start()
            l_copy(g, me_z).start()

        @pl.when(g == me_z)
        def _():
            o_copy(g, 1 - core).start()
            pltpu.make_async_copy(os.at[g, core], oland.at[core * NZ + me_z], own_out_sem.at[0]).start()
            pltpu.make_async_copy(ls.at[g], lland.at[me_z], own_out_sem.at[1]).start()

        return carry

    stat[...] = jnp.zeros_like(stat)
    os[...] = jnp.zeros_like(os)
    lax.fori_loop(0, NZ, attend_group, 0)

    def o_arrival(head):
        return pltpu.make_async_remote_copy(
            src_ref=os.at[0, 0], dst_ref=oland.at[head], send_sem=o_send.at[0, 0],
            recv_sem=o_recv.at[head], device_id={"tp": 1 - core}, device_id_type=MESH,
        )

    pltpu.make_async_copy(os.at[me_z, core], oland.at[core * NZ + me_z], own_out_sem.at[0]).wait()
    pltpu.make_async_copy(ls.at[me_z], lland.at[me_z], own_out_sem.at[1]).wait()
    for t in range(1, NZ):
        z = order(t, me_z)
        o_arrival(core * NZ + z).wait_recv()
        l_copy(z, z).wait_recv()
    for z in range(NZ):
        o_arrival((1 - core) * NZ + z).wait_recv()
    low128 = lane_iota < HEAD_DIM
    for i in range(NZ):
        a, b = oland[2 * i].astype(F32), oland[2 * i + 1].astype(F32)
        cols = pl.ds(i * 128, 128)
        att[0:128, cols] = jnp.where(low128, a, pltpu.roll(b, HEAD_DIM, 1)).astype(BF16)
        att[128:256, cols] = jnp.where(low128, pltpu.roll(a, HEAD_DIM, 1), b).astype(BF16)
    low8 = low128[:8]
    for h in range(NZ):
        mine = lland[h]
        turned = pltpu.roll(mine, HEAD_DIM, 1)
        for q, (left, right) in enumerate(
            ((mine[0:1], turned[1:2]), (mine[2:3], turned[3:4]), (turned[0:1], mine[1:2]), (turned[2:3], mine[3:4]))
        ):
            logs_ref[h:h + 1, q * 128:(q + 1) * 128] = jnp.where(low8[:1], left, right)
    wo_local.wait()
    wo_remote.wait_send()
    pltpu.make_async_remote_copy(
        src_ref=wo_hbm, dst_ref=wo.at[pl.ds((1 - core) * wo_rows, wo_rows)], send_sem=wo_send, recv_sem=wo_recv,
        device_id={"tp": 1 - core}, device_id_type=MESH,
    ).wait_recv()

    def project_out(n, carry):
        cols = pl.ds(pl.multiple_of(n * 512, 512), 512)
        out_ref[:, cols] = jnp.dot(att[...], wo[:, cols], preferred_element_type=F32).astype(BF16)
        return carry

    lax.fori_loop(0, out_ref.shape[1] // 512, project_out, 0)

    for t in range(1, NZ):
        z = order(t, me_z)
        kv_copy(z).wait_send()
        q_copy(z, me_z).wait_send()
        c_copy(z, me_z).wait_send()
        o_copy(z, 0).wait_send()
        o_copy(z, 1).wait_send()
        l_copy(z, me_z).wait_send()
    o_copy(me_z, 1 - core).wait_send()
    for z in range(NZ):
        for way in range(2):
            y_copy(z, way).wait_send()
            f_copy(z, way).wait_send()


def on_device(tokens, w_query, w_key, w_value, w_out, chosen):
    rows, model = tokens.shape[1:]
    width = w_query.shape[1]
    hbm = pl.BlockSpec(memory_space=pl.ANY)
    vmem = pl.BlockSpec(memory_space=pltpu.VMEM)
    dma = pltpu.SemaphoreType.DMA
    mixed, log_sums = pl.pallas_call(
        kernel,
        out_shape=(
            jax.ShapeDtypeStruct((rows // 2, model), BF16),
            jax.ShapeDtypeStruct((width // HEAD_DIM, rows), F32),
        ),
        in_specs=[hbm] * 5 + [vmem],
        out_specs=(vmem, vmem),
        scratch_shapes=[
            pltpu.VMEM((rows, model), BF16),
            pltpu.VMEM((4, model, 256), BF16),
            pltpu.VMEM((model, width), BF16),
            pltpu.VMEM((2 * width, model), BF16),
            pltpu.VMEM((NZ, rows // BLOCK, BLOCK, 128), BF16),
            pltpu.VMEM((NZ * NY * rows // BLOCK, BLOCK, 128), BF16),
            pltpu.VMEM((NZ, rows // 2, 128), BF16),
            pltpu.VMEM((NZ, rows // 2, 128), BF16),
            pltpu.VMEM((8, 128), jnp.int32),
            pltpu.VMEM((NZ, 8, 128), jnp.int32),
            pltpu.SMEM((NZ, 8, 128), jnp.int32),
            pltpu.VMEM((PICKS * BLOCK, 256), BF16),
            pltpu.VMEM((NZ, 2, 128, 128), BF16),
            pltpu.VMEM((2 * NZ, 128, 128), BF16),
            pltpu.VMEM((128, 128), F32),
            pltpu.VMEM((NZ, 8, 128), F32),
            pltpu.VMEM((NZ, 8, 128), F32),
            pltpu.VMEM((rows // 2, 2 * width), BF16),
            dma((10,)), dma, dma, dma, dma((3,)), dma((2,)), dma,
            dma((NZ,)), dma((NZ,)), dma((NZ,)), dma((NZ,)), dma((NZ,)), dma((NZ,)),
            dma((NZ, 2)), dma((NZ, 2)), dma((NZ, 2)), dma((NZ, 2)),
            dma((NZ, 2)), dma((2 * NZ,)), dma((NZ,)), dma((NZ,)),
        ],
        compiler_params=pltpu.CompilerParams(collective_id=0, has_side_effects=True, vmem_limit_bytes=48 * 2**20),
        name="heads_over_z",
    )(tokens[0], w_query, w_key, w_value, w_out, chosen[0])
    return mixed[None], log_sums[None]


def solution(mesh):
    return jax.shard_map(
        on_device,
        mesh=mesh,
        in_specs=(
            P("dp", "kv", None),
            P(None, "tp"),
            P(None, "tp"),
            P(None, "tp"),
            P("tp", None),
            P("dp", "kv", None),
        ),
        out_specs=(P("dp", ("kv", "tp"), None), P("dp", "tp", "kv")),
        check_vma=False,
    )
```

time: 344 us -> 94.9 us (0.28)
  blocking collectives: 98.8 us -> 0 us
  Pallas kernels: 0 us -> 88.6 us
  local copies, waits for them, and re-layouts: 87.9 us -> 5.44 us
  matrix products: 51 us -> 0 us
  other arithmetic: 40.1 us -> 0 us
  waiting for transfers between devices: 36.4 us -> 0 us
  starting transfers between devices: 26.2 us -> 0 us
    all_to_all x1 -> x0, blocking collectives: 98.8 us -> none  [on_device(): lax.all_to_all(send_keys, 'kv', split_axis=0, concat_axis=0, tiled=True)]
    pallas_call x0 -> x1, Pallas kernels: none -> 88.6 us  [on_device(): pl.pallas_call(kernel, out_shape=(jax.ShapeDtypeStruct((rows // 2, model)...]
    reshape x5 -> x0, local copies, waits for them, and re-layouts: 61.4 us -> none  [the longest x2 36.4 us: on_device(): pool_keys[slots].reshape(query_count, picks, BLOCK, head_count, HEAD_DIM)]
    all_to_all x3 -> x0, waiting for transfers between devices: 36.4 us -> none  [the longest x1 30.8 us: on_device(): lax.all_to_all(send_values, 'kv', split_axis=0, concat_axis=0, tiled=True)]
    dot_general x5 -> x0, matrix products: 33.2 us -> none  [the longest x1 20.5 us: on_device(): jnp.einsum('nhqsk,nskhd->nqhd', weights, values_sel, preferred_element_ty...]
    all_to_all x3 -> x0, starting transfers between devices: 26.2 us -> none  [the longest x1 12 us: on_device(): lax.all_to_all(wanted, 'kv', split_axis=0, concat_axis=0, tiled=True)]
    gather x4 -> x0, local copies, waits for them, and re-layouts: 22.9 us -> none  [the longest x1 8.69 us: on_device(): pool_values[slots].reshape(query_count, picks, BLOCK, head_count, HEAD_DIM)]
    reduce_sum x4 -> x0, other arithmetic: 20.7 us -> none  [the longest x1 14.7 us: on_device(): row_sum = jnp.sum(exp_terms, axis=(3, 4), keepdims=True)]
  transfers between devices with their start and end apart: 3 -> 0, of which waited for: 3 -> 0; matrix products, arithmetic and copies ran while one was open for 20% -> 0% of each run, Pallas kernels for 0% -> 0%
where the time goes in v1:
time: 94.9 us; the launch traced here: 94.7 us
  Pallas kernels  88.6 us (93%)
  local copies, waits for them, and re-layouts  5.44 us (6%)
    pallas_call x1, Pallas kernels, on_device(): pl.pallas_call(kernel, out_shape=(jax.ShapeDtypeStruct((rows // 2, model)...  88.6 us
    unnamed x8, local copies, waits for them, and re-layouts  5.44 us

profile of v1, /device:TPU:1, one launch (start us, length us, event | category | flops | bytes accessed | tf_op | source)
XLA Modules:
  0.0 94.7 jit_solution(2035925152684680489)
XLA Ops:
  0.6 0.0 copy-start
  0.6 1.6 %copy-done = bf16[1,512,2048]{2,1,0:T(8,128)(2,1)S(1)} copy-done((bf16[1,512,2048]{2,1,0:T(8,128)(2,1)S(1)}, bf16[1,512,2048]{2,1,0:T(8,128)(2,1)}, u32[]{:S(2)}) %copy-start) | copy-done | bytes 2097176
  2.2 0.0 copy-start.1
  2.2 1.6 %copy-done.1 = bf16[2048,512]{1,0:T(8,128)(2,1)S(1)} copy-done((bf16[2048,512]{1,0:T(8,128)(2,1)S(1)}, bf16[2048,512]{1,0:T(8,128)(2,1)}, u32[]{:S(2)}) %copy-start.1) | copy-done | bytes 2097176
  3.8 0.0 copy-start.2
  3.8 0.7 copy-done.2
  4.5 88.6 %heads_over_z.1 = (bf16[256,2048]{1,0:T(8,128)(2,1)S(1)}, f32[8,512]{1,0:T(8,128)S(1)}) custom-call(bf16[512,2048]{1,0:T(8,128)(2,1)S(1)} %bitcast.4, bf16[2048,512]{1,0:T(8,128)(2,1)S(1)} %copy-done.1, bf16[2048,512]{1,0:T(8,128)(2,1)} %wk_hbm.1, bf16[2048,512]{1,0:T(8,128)(2,1)} %wv_hbm.1, bf16[512,2048]{1,0:T(8,128)(2,1)} %wo_hbm.1, s32[8,16]{1,0:T(8,128)S(1)} %bitcast.7), custom_call_target="tpu_custom_call" | custom-call | tf_op jit(solution)/shard_map/heads_over_z/pallas_call | solution.py:349
  93.1 1.0 %copy.10 = bf16[1,256,2048]{2,1,0:T(8,128)(2,1)} copy(bf16[1,256,2048]{2,1,0:T(8,128)(2,1)S(1)} %bitcast.5) | data formatting | bytes 2097152
  94.1 0.6 copy.11
Async XLA Ops:
  0.6 1.6 %copy-start = (bf16[1,512,2048]{2,1,0:T(8,128)(2,1)S(1)}, bf16[1,512,2048]{2,1,0:T(8,128)(2,1)}, u32[]{:S(2)}) copy-start(bf16[1,512,2048]{2,1,0:T(8,128)(2,1)} %param.6) | copy-start | bytes 6291460
  2.2 1.6 %copy-start.1 = (bf16[2048,512]{1,0:T(8,128)(2,1)S(1)}, bf16[2048,512]{1,0:T(8,128)(2,1)}, u32[]{:S(2)}) copy-start(bf16[2048,512]{1,0:T(8,128)(2,1)} %wq_hbm.1) | copy-start | bytes 6291460
  3.8 0.7 copy-start.2

commit v2 on v1

--- a/solution.py
+++ b/solution.py
@@ -18,17 +18,23 @@
 F32 = jnp.float32
 
 
-def order(step, me_z):
-    half = (step + 1) // 2
-    return lax.rem(me_z + jnp.where(lax.rem(step, 2) == 1, half, NZ - half), NZ)
+def arrival_order(step, me_z):
+    turn = step // 2
+    second = step - 2 * turn
+    parity = lax.rem(me_z, 2)
+    pair = lax.rem(me_z // 2 + jnp.where(turn == 1, 3, jnp.where(turn == 2, 1, jnp.where(turn == 3, 2, 0))), NZ // 2)
+    swapped = lax.rem(parity + 1 - second + NZ, 2)
+    straight = lax.rem(parity + second, 2)
+    member = jnp.where(turn == 0, straight, jnp.where(turn == 1, 1 - second, jnp.where(turn == 2, second, swapped)))
+    return pair * 2 + member
 
 
 def kernel(
     x_hbm, wq_hbm, wk_hbm, wv_hbm, wo_hbm, chosen_ref, out_ref, logs_ref,
-    x, wkv, wq, wo, kvs, land, qs, qland, cs, cland, picks, gathered, os, oland, stat, ls, lland, att,
+    x, wkv, wq, wo, kvs, land, qs, qland, cs, cland, picks, relay_kv, relay_q, scores, os, oland, stat, ls, lland, att,
     in_sem, wo_sem, wo_send, wo_recv, own_sem, own_out_sem, pick_sem,
     kv_send, kv_recv, q_send, q_recv, c_send, c_recv,
-    y_send, y_recv, f_send, f_recv, o_send, o_recv, l_send, l_recv,
+    relay_send, relay_recv, y_send, y_recv, f_send, f_recv, o_send, o_recv, l_send, l_recv,
 ):
     kv = lax.axis_index("kv")
     core = lax.axis_index("tp")
@@ -47,15 +53,16 @@
     x_copy = pltpu.make_async_copy(x_hbm, x, in_sem.at[0])
     x_copy.start()
     w_copies = []
-    for p in range(4):
-        pair = []
+    for n, turn in enumerate((0, 1, 3, 2)):
+        pair = lax.rem(me_z // 2 + turn, NZ // 2)
+        cols = pl.ds(pl.multiple_of(pair * 128, 128), 128)
+        copies = []
         for i, src in enumerate((wk_hbm, wv_hbm)):
-            c = pltpu.make_async_copy(
-                src.at[:, pl.ds(p * 128, 128)], wkv.at[p, :, pl.ds(i * 128, 128)], in_sem.at[1 + 2 * p + i]
+            copies.append(
+                pltpu.make_async_copy(src.at[:, cols], wkv.at[n, :, pl.ds(i * 128, 128)], in_sem.at[1 + 2 * n + i])
             )
-            c.start()
-            pair.append(c)
-        w_copies.append(pair)
+            copies[-1].start()
+        w_copies.append((pair, copies))
     wq_copy = pltpu.make_async_copy(wq_hbm, wq, in_sem.at[9])
     wq_copy.start()
 
@@ -75,20 +82,9 @@
     lane = lax.broadcasted_iota(jnp.int32, (rows, 128), 1)
     low = lane < HEAD_DIM
 
-    x_copy.wait()
-    for p in range(4):
-        for c in w_copies[p]:
-            c.wait()
-
-    def project_pair(p, carry):
-        both = jnp.dot(x[...], wkv[p], preferred_element_type=F32)
-        kp, vp = both[:, 0:128], both[:, 128:256]
-        kvs[2 * p] = jnp.where(low, kp, pltpu.roll(vp, HEAD_DIM, 1)).astype(BF16).reshape(blocks, BLOCK, 128)
-        kvs[2 * p + 1] = jnp.where(low, pltpu.roll(kp, HEAD_DIM, 1), vp).astype(BF16).reshape(blocks, BLOCK, 128)
-        return carry
-
-    lax.fori_loop(0, 4, project_pair, 0)
-    pl.semaphore_wait(barrier, 2 * NZ + 1)
+    far = lax.rem(me_z + NZ // 2, NZ)
+    left = lax.rem(me_z + NZ - 1, NZ)
+    right = lax.rem(me_z + 1, NZ)
 
     def kv_copy(z):
         return pltpu.make_async_remote_copy(
@@ -114,14 +110,70 @@
             recv_sem=c_recv.at[src], device_id={"kv": at(z)}, device_id_type=MESH,
         )
 
+    def kv_first_leg():
+        return pltpu.make_async_remote_copy(
+            src_ref=kvs.at[far], dst_ref=relay_kv, send_sem=kv_send.at[far],
+            recv_sem=relay_recv.at[0], device_id={"kv": at(left)}, device_id_type=MESH,
+        )
+
+    def kv_second_leg():
+        return pltpu.make_async_remote_copy(
+            src_ref=relay_kv, dst_ref=land.at[pl.ds(at(right) * blocks, blocks)], send_sem=relay_send.at[0],
+            recv_sem=kv_recv.at[right], device_id={"kv": at(lax.rem(right + NZ // 2, NZ))}, device_id_type=MESH,
+        )
+
+    def q_first_leg():
+        return pltpu.make_async_remote_copy(
+            src_ref=qs.at[far], dst_ref=relay_q, send_sem=q_send.at[far],
+            recv_sem=relay_recv.at[1], device_id={"kv": at(left)}, device_id_type=MESH,
+        )
+
+    def q_second_leg():
+        return pltpu.make_async_remote_copy(
+            src_ref=relay_q, dst_ref=qland.at[right], send_sem=relay_send.at[1],
+            recv_sem=q_recv.at[right], device_id={"kv": at(lax.rem(right + NZ // 2, NZ))}, device_id_type=MESH,
+        )
+
+    def y_copy(z, way, src=None):
+        rng = pl.ds(at(z) * blocks, blocks)
+        return pltpu.make_async_remote_copy(
+            src_ref=land.at[rng] if src is None else src, dst_ref=land.at[rng], send_sem=y_send.at[z, way],
+            recv_sem=y_recv.at[z, way], device_id={"kv": (up, down)[way]}, device_id_type=MESH,
+        )
+
     own_kv = pltpu.make_async_copy(kvs.at[me_z], land.at[pl.ds(kv * blocks, blocks)], own_sem.at[0])
-    own_kv.start()
     own_c = pltpu.make_async_copy(cs, cland.at[me_z], own_sem.at[1])
-    own_c.start()
-    for t in range(1, NZ):
-        c_copy(order(t, me_z), me_z).start()
-    for t in range(1, NZ):
-        kv_copy(order(t, me_z)).start()
+    x_copy.wait()
+    parity = lax.rem(me_z, 2)
+    for n, (pair, copies) in enumerate(w_copies):
+        for c in copies:
+            c.wait()
+        both = jnp.dot(x[...], wkv[n], preferred_element_type=F32)
+        kp, vp = both[:, 0:128], both[:, 128:256]
+        kvs[2 * pair] = jnp.where(low, kp, pltpu.roll(vp, HEAD_DIM, 1)).astype(BF16).reshape(blocks, BLOCK, 128)
+        kvs[2 * pair + 1] = jnp.where(low, pltpu.roll(kp, HEAD_DIM, 1), vp).astype(BF16).reshape(blocks, BLOCK, 128)
+        if n == 0:
+            pl.semaphore_wait(barrier, 2 * NZ + 1)
+            own_c.start()
+            for t in range(1, NZ):
+                c_copy(arrival_order(t, me_z), me_z).start()
+            for way in range(2):
+                y_copy(me_z, way, kvs.at[me_z]).start()
+            own_kv.start()
+            kv_copy(2 * pair + 1 - parity).start()
+        elif n < 3:
+            for m in ((0, 1) if n == 1 else (1, 0)):
+                kv_copy(2 * pair + m).start()
+        else:
+            @pl.when(core == 0)
+            def _():
+                kv_copy(far).start()
+
+            @pl.when(core == 1)
+            def _():
+                kv_first_leg().start()
+
+            kv_copy(2 * pair + 1 - parity).start()
 
     wo_rows = wo_hbm.shape[0]
     wo_mine = wo.at[pl.ds(core * wo_rows, wo_rows)]
@@ -147,23 +199,25 @@
     lax.fori_loop(0, 2, project_queries, 0)
     own_q = pltpu.make_async_copy(qs.at[me_z], qland.at[me_z], own_sem.at[2])
     own_q.start()
-    for t in range(1, NZ):
-        q_copy(order(t, me_z), me_z).start()
-
-    def y_copy(z, way):
-        rng = pl.ds(at(z) * blocks, blocks)
+
+    @pl.when(core == 0)
+    def _():
+        q_copy(far, me_z).start()
+
+    @pl.when(core == 1)
+    def _():
+        q_first_leg().start()
+
+    for t in range(6, 0, -1):
+        q_copy(arrival_order(t, me_z), me_z).start()
+
+    def y_arrival(z, way):
+        rng = pl.ds((z * NY + (below, above)[way]) * blocks, blocks)
         return pltpu.make_async_remote_copy(
             src_ref=land.at[rng], dst_ref=land.at[rng], send_sem=y_send.at[z, way],
             recv_sem=y_recv.at[z, way], device_id={"kv": (up, down)[way]}, device_id_type=MESH,
         )
 
-    def y_arrival(z, way):
-        rng = pl.ds((z * NY + (below, above)[way]) * blocks, blocks)
-        return pltpu.make_async_remote_copy(
-            src_ref=land.at[rng], dst_ref=land.at[rng], send_sem=y_send.at[z, way],
-            recv_sem=y_recv.at[z, way], device_id={"kv": (up, down)[way]}, device_id_type=MESH,
-        )
-
     def f_copy(z, way):
         rng = pl.ds((z * NY + (below, above)[way]) * blocks + way * (blocks // 2), blocks // 2)
         return pltpu.make_async_remote_copy(
@@ -171,28 +225,36 @@
             recv_sem=f_recv.at[z, way], device_id={"kv": (up, down)[way]}, device_id_type=MESH,
         )
 
-    far = lax.rem(me_y + 2, NY)
+    across = lax.rem(me_y + 2, NY)
 
     def f_arrival(z, way):
-        rng = pl.ds((z * NY + far) * blocks + way * (blocks // 2), blocks // 2)
+        rng = pl.ds((z * NY + across) * blocks + way * (blocks // 2), blocks // 2)
         return pltpu.make_async_remote_copy(
             src_ref=land.at[rng], dst_ref=land.at[rng], send_sem=f_send.at[z, way],
             recv_sem=f_recv.at[z, way], device_id={"kv": (up, down)[way]}, device_id_type=MESH,
         )
 
     own_kv.wait()
-    for t in range(NZ + 1):
+    for t in range(1, NZ + 1):
         if t < NZ:
-            z = order(t, me_z)
-            if t > 0:
-                kv_arrival(z).wait_recv()
+            z = arrival_order(t, me_z)
+            kv_arrival(z).wait_recv()
             for way in range(2):
                 y_copy(z, way).start()
-        if t > 0:
-            z = order(t - 1, me_z)
-            for way in range(2):
-                y_arrival(z, way).wait_recv()
-                f_copy(z, way).start()
+        z = arrival_order(t - 1, me_z)
+        for way in range(2):
+            y_arrival(z, way).wait_recv()
+            f_copy(z, way).start()
+        if t == 5:
+            @pl.when(core == 1)
+            def _():
+                kv_first_leg().wait_recv()
+                kv_second_leg().start()
+        if t == 6:
+            @pl.when(core == 1)
+            def _():
+                q_first_leg().wait_recv()
+                q_second_leg().start()
     for z in range(NZ):
         for way in range(2):
             f_arrival(z, way).wait_recv()
@@ -200,18 +262,14 @@
     own_c.wait()
     own_q.wait()
     for t in range(1, NZ):
-        z = order(t, me_z)
+        z = arrival_order(t, me_z)
         c_copy(z, z).wait_recv()
     to_scalars = pltpu.make_async_copy(cland, picks, pick_sem)
     to_scalars.start()
     to_scalars.wait()
 
-    row_iota = lax.broadcasted_iota(jnp.int32, (128, 128), 0)
     lane_iota = lax.broadcasted_iota(jnp.int32, (128, 128), 1)
     low64 = lax.broadcasted_iota(jnp.int32, (BLOCK, 128), 1) < HEAD_DIM
-    key_iota = lax.broadcasted_iota(jnp.int32, (128, PICKS * BLOCK), 1)
-    row_col = lax.broadcasted_iota(jnp.int32, (128, 1), 0)
-    hidden = (lane_iota < BLOCK) & (lane_iota > lax.rem(row_iota, BLOCK))
     zero = jnp.zeros((BLOCK, 128), BF16)
 
     def o_copy(g, to):
@@ -226,43 +284,61 @@
             recv_sem=l_recv.at[src], device_id={"kv": at(g)}, device_id_type=MESH,
         )
 
-    def attend_group(t, carry):
-        g = order(t, me_z)
-
-        @pl.when(t > 0)
-        def _():
-            q_copy(g, g).wait_recv()
-
-        def attend_pair(j, carry):
-            for s in range(PICKS):
-                for i in range(2):
-                    gathered[pl.ds(s * BLOCK, BLOCK), pl.ds(i * 128, 128)] = land[picks[g, j + 4 * i, s]]
-            tile = qland[g, pl.ds(pl.multiple_of(j * BLOCK, BLOCK), BLOCK), :].astype(F32)
-            first = jnp.where(low64, tile, 0.0).astype(BF16)
-            second = jnp.where(low64, pltpu.roll(tile, HEAD_DIM, 1), 0.0).astype(BF16)
-            lhs = jnp.concatenate(
-                [jnp.concatenate([first, zero], axis=1), jnp.concatenate([zero, second], axis=1)], axis=0
-            )
-            s = lax.dot_general(lhs, gathered[...], (((1,), (1,)), ((), ())), preferred_element_type=F32)
-            device = g * NY + me_y
-            limit = (jnp.where(row_col < BLOCK, j, j + 4) + 2 * device + 1) * BLOCK
-            s = jnp.where(key_iota < limit, s, -jnp.inf)
-            s = jnp.concatenate([jnp.where(hidden, -jnp.inf, s[:, 0:128]), s[:, 128:]], axis=1)
+    key_row = lax.broadcasted_iota(jnp.int32, (1, PICKS * BLOCK), 1)
+    diagonal = jnp.where(
+        lax.broadcasted_iota(jnp.int32, (BLOCK, 128), 1) >= BLOCK, 0.0,
+        jnp.where(
+            lax.broadcasted_iota(jnp.int32, (BLOCK, 128), 1) > lax.broadcasted_iota(jnp.int32, (BLOCK, 128), 0),
+            -jnp.inf, 0.0,
+        ),
+    )
+
+    def listed(g, j):
+        return jnp.concatenate([land[picks[g, j, s]] for s in range(PICKS)], axis=0)
+
+    def score(g, j, slot):
+        tile = qland[g, j * BLOCK:(j + 1) * BLOCK, :].astype(F32)
+        halves = (tile, pltpu.roll(tile, HEAD_DIM, 1))
+        first, second = [jnp.where(low64, h, 0.0).astype(BF16) for h in halves]
+        lhs = jnp.concatenate([jnp.concatenate([first, zero], axis=1), jnp.concatenate([zero, second], axis=1)], axis=0)
+        keys = jnp.concatenate([listed(g, j), listed(g, j + 4)], axis=1)
+        res = lax.dot_general(lhs, keys, (((1,), (1,)), ((), ())), preferred_element_type=F32)
+        scores[slot, 0] = res[:BLOCK]
+        scores[slot, 1] = res[BLOCK:]
+
+    def finish(g, j, slot):
+        device = g * NY + me_y
+        for i in range(2):
+            bias = jnp.where(key_row < (j + 4 * i + 2 * device + 1) * BLOCK, 0.0, -jnp.inf)
+            s = scores[slot, i] + bias
+            s = jnp.concatenate([s[:, 0:128] + diagonal, s[:, 128:]], axis=1)
             peak = jnp.max(s, axis=1, keepdims=True)
             e = jnp.exp2((s - peak) * (LOG2E * HEAD_DIM ** -0.5))
             total = jnp.sum(e, axis=1, keepdims=True)
-            o = jnp.dot(e.astype(BF16), gathered[...], preferred_element_type=F32) * (1.0 / total)
+            part = jnp.dot(e.astype(BF16), listed(g, j + 4 * i), preferred_element_type=F32) * (1.0 / total)
             log_sum = peak * HEAD_DIM ** -0.5 + jnp.log(total)
-            stat[...] = jnp.where(lane_iota == j, log_sum, stat[...])
-            place = pl.ds(pl.multiple_of(lax.rem(j, 2) * BLOCK, BLOCK), BLOCK)
-            for i in range(2):
-                part = o[i * BLOCK:(i + 1) * BLOCK, i * 128:(i + 1) * 128]
-                old = os[g, i, place, :].astype(F32)
-                left = jnp.where(j < 2, pltpu.roll(part, HEAD_DIM, 1), old)
-                os[g, i, place, :] = jnp.where(low64, left, part).astype(BF16)
-            return carry
-
-        lax.fori_loop(0, 4, attend_pair, 0)
+            band = slice(i * BLOCK, (i + 1) * BLOCK)
+            stat[band, :] = jnp.where(lane_iota[band] == j, log_sum, stat[band, :])
+            place = slice((j % 2) * BLOCK, (j % 2 + 1) * BLOCK)
+            if j < 2:
+                os[g, i, place, :] = pltpu.roll(part, HEAD_DIM, 1).astype(BF16)
+            else:
+                os[g, i, place, :] = jnp.where(low64, os[g, i, place, :].astype(F32), part).astype(BF16)
+
+    def attend_group(t, carry):
+        g = arrival_order(NZ - 1 - t, me_z)
+        following = arrival_order(jnp.maximum(NZ - 2 - t, 0), me_z)
+
+        @pl.when(t < NZ - 2)
+        def _():
+            q_copy(following, following).wait_recv()
+
+        for j in range(4):
+            if j < 3:
+                score(g, j + 1, (j + 1) % 2)
+            else:
+                score(following, 0, 0)
+            finish(g, j, j % 2)
         ls[g] = stat[...].T[0:8]
 
         @pl.when(g != me_z)
@@ -281,6 +357,8 @@
 
     stat[...] = jnp.zeros_like(stat)
     os[...] = jnp.zeros_like(os)
+    q_copy(far, far).wait_recv()
+    score(far, 0, 0)
     lax.fori_loop(0, NZ, attend_group, 0)
 
     def o_arrival(head):
@@ -292,7 +370,7 @@
     pltpu.make_async_copy(os.at[me_z, core], oland.at[core * NZ + me_z], own_out_sem.at[0]).wait()
     pltpu.make_async_copy(ls.at[me_z], lland.at[me_z], own_out_sem.at[1]).wait()
     for t in range(1, NZ):
-        z = order(t, me_z)
+        z = arrival_order(t, me_z)
         o_arrival(core * NZ + z).wait_recv()
         l_copy(z, z).wait_recv()
     for z in range(NZ):
@@ -307,10 +385,10 @@
     for h in range(NZ):
         mine = lland[h]
         turned = pltpu.roll(mine, HEAD_DIM, 1)
-        for q, (left, right) in enumerate(
+        for q, (one, other) in enumerate(
             ((mine[0:1], turned[1:2]), (mine[2:3], turned[3:4]), (turned[0:1], mine[1:2]), (turned[2:3], mine[3:4]))
         ):
-            logs_ref[h:h + 1, q * 128:(q + 1) * 128] = jnp.where(low8[:1], left, right)
+            logs_ref[h:h + 1, q * 128:(q + 1) * 128] = jnp.where(low8[:1], one, other)
     wo_local.wait()
     wo_remote.wait_send()
     pltpu.make_async_remote_copy(
@@ -326,7 +404,7 @@
     lax.fori_loop(0, out_ref.shape[1] // 512, project_out, 0)
 
     for t in range(1, NZ):
-        z = order(t, me_z)
+        z = arrival_order(t, me_z)
         kv_copy(z).wait_send()
         q_copy(z, me_z).wait_send()
         c_copy(z, me_z).wait_send()
@@ -334,6 +412,12 @@
         o_copy(z, 1).wait_send()
         l_copy(z, me_z).wait_send()
     o_copy(me_z, 1 - core).wait_send()
+
+    @pl.when(core == 1)
+    def _():
+        kv_second_leg().wait_send()
+        q_second_leg().wait_send()
+
     for z in range(NZ):
         for way in range(2):
             y_copy(z, way).wait_send()
@@ -366,7 +450,9 @@
             pltpu.VMEM((8, 128), jnp.int32),
             pltpu.VMEM((NZ, 8, 128), jnp.int32),
             pltpu.SMEM((NZ, 8, 128), jnp.int32),
-            pltpu.VMEM((PICKS * BLOCK, 256), BF16),
+            pltpu.VMEM((rows // BLOCK, BLOCK, 128), BF16),
+            pltpu.VMEM((rows // 2, 128), BF16),
+            pltpu.VMEM((2, 2, BLOCK, PICKS * BLOCK), F32),
             pltpu.VMEM((NZ, 2, 128, 128), BF16),
             pltpu.VMEM((2 * NZ, 128, 128), BF16),
             pltpu.VMEM((128, 128), F32),
@@ -375,10 +461,10 @@
             pltpu.VMEM((rows // 2, 2 * width), BF16),
             dma((10,)), dma, dma, dma, dma((3,)), dma((2,)), dma,
             dma((NZ,)), dma((NZ,)), dma((NZ,)), dma((NZ,)), dma((NZ,)), dma((NZ,)),
-            dma((NZ, 2)), dma((NZ, 2)), dma((NZ, 2)), dma((NZ, 2)),
+            dma((2,)), dma((2,)), dma((NZ, 2)), dma((NZ, 2)), dma((NZ, 2)), dma((NZ, 2)),
             dma((NZ, 2)), dma((2 * NZ,)), dma((NZ,)), dma((NZ,)),
         ],
-        compiler_params=pltpu.CompilerParams(collective_id=0, has_side_effects=True, vmem_limit_bytes=48 * 2**20),
+        compiler_params=pltpu.CompilerParams(collective_id=0, has_side_effects=True, vmem_limit_bytes=62 * 2**20),
         name="heads_over_z",
     )(tokens[0], w_query, w_key, w_value, w_out, chosen[0])
     return mixed[None], log_sums[None]

time: 94.9 us -> 81.3 us (0.86)
  Pallas kernels: 88.6 us -> 77.6 us
  local copies, waits for them, and re-layouts: 5.44 us -> 2.92 us
    pallas_call x1, Pallas kernels: 88.6 us -> 77.6 us  [on_device(): pl.pallas_call(kernel, out_shape=(jax.ShapeDtypeStruct((rows // 2, model)...]
    unnamed x8 -> x4, local copies, waits for them, and re-layouts: 5.44 us -> 2.92 us
where the time goes in v2:
time: 81.3 us; the launch traced here: 81.2 us
  Pallas kernels  77.6 us (95%)
  local copies, waits for them, and re-layouts  2.92 us (4%)
    pallas_call x1, Pallas kernels, on_device(): pl.pallas_call(kernel, out_shape=(jax.ShapeDtypeStruct((rows // 2, model)...  77.6 us
    unnamed x4, local copies, waits for them, and re-layouts  2.92 us

profile of v2, /device:TPU:1, one launch (start us, length us, event | category | flops | bytes accessed | tf_op | source)
XLA Modules:
  0.0 81.2 jit_solution(9818466886787737068)
XLA Ops:
  0.6 77.6 %heads_over_z.1 = (bf16[256,2048]{1,0:T(8,128)(2,1)}, f32[8,512]{1,0:T(8,128)}) custom-call(bf16[512,2048]{1,0:T(8,128)(2,1)} %bitcast.4, bf16[2048,512]{1,0:T(8,128)(2,1)} %wq_hbm.1, bf16[2048,512]{1,0:T(8,128)(2,1)} %wk_hbm.1, bf16[2048,512]{1,0:T(8,128)(2,1)} %wv_hbm.1, bf16[512,2048]{1,0:T(8,128)(2,1)} %wo_hbm.1, s32[8,16]{1,0:T(8,128)} %bitcast.7), custom_call_target="tpu_custom_call" | custom-call | tf_op jit(solution)/shard_map/heads_over_z/pallas_call | solution.py:433
  78.2 0.0 copy-start
  78.3 2.3 %copy.10 = bf16[1,256,2048]{2,1,0:T(8,128)(2,1)} copy(bf16[1,256,2048]{2,1,0:T(8,128)(2,1)} %bitcast.5) | data formatting | bytes 2097152
  80.6 0.0 copy-done
  80.6 0.6 copy.11
Async XLA Ops:
  78.2 2.3 %copy-start = (f32[8,512]{1,0:T(8,128)S(1)}, f32[8,512]{1,0:T(8,128)}, u32[]{:S(2)}) copy-start(f32[8,512]{1,0:T(8,128)} %get-tuple-element.5) | copy-start | bytes 49156

commit v3 on v2

--- a/solution.py
+++ b/solution.py
@@ -19,22 +19,18 @@
 
 
 def arrival_order(step, me_z):
-    turn = step // 2
-    second = step - 2 * turn
-    parity = lax.rem(me_z, 2)
-    pair = lax.rem(me_z // 2 + jnp.where(turn == 1, 3, jnp.where(turn == 2, 1, jnp.where(turn == 3, 2, 0))), NZ // 2)
-    swapped = lax.rem(parity + 1 - second + NZ, 2)
-    straight = lax.rem(parity + second, 2)
-    member = jnp.where(turn == 0, straight, jnp.where(turn == 1, 1 - second, jnp.where(turn == 2, second, swapped)))
-    return pair * 2 + member
+    distance = (step + 1) // 2
+    onward = lax.rem(me_z + step, 2) == 1
+    offset = jnp.where(onward, distance, NZ - distance)
+    return lax.rem(me_z + offset, NZ)
 
 
 def kernel(
     x_hbm, wq_hbm, wk_hbm, wv_hbm, wo_hbm, chosen_ref, out_ref, logs_ref,
-    x, wkv, wq, wo, kvs, land, qs, qland, cs, cland, picks, relay_kv, relay_q, scores, os, oland, stat, ls, lland, att,
+    x, wkv, wq, wo, kvs, land, qs, qland, cs, cland, picks, scores, os, oland, stat, ls, lland, att,
     in_sem, wo_sem, wo_send, wo_recv, own_sem, own_out_sem, pick_sem,
     kv_send, kv_recv, q_send, q_recv, c_send, c_recv,
-    relay_send, relay_recv, y_send, y_recv, f_send, f_recv, o_send, o_recv, l_send, l_recv,
+    y_send, y_recv, f_send, f_recv, o_send, o_recv, l_send, l_recv,
 ):
     kv = lax.axis_index("kv")
     core = lax.axis_index("tp")
@@ -50,22 +46,6 @@
     def at(z):
         return z * NY + me_y
 
-    x_copy = pltpu.make_async_copy(x_hbm, x, in_sem.at[0])
-    x_copy.start()
-    w_copies = []
-    for n, turn in enumerate((0, 1, 3, 2)):
-        pair = lax.rem(me_z // 2 + turn, NZ // 2)
-        cols = pl.ds(pl.multiple_of(pair * 128, 128), 128)
-        copies = []
-        for i, src in enumerate((wk_hbm, wv_hbm)):
-            copies.append(
-                pltpu.make_async_copy(src.at[:, cols], wkv.at[n, :, pl.ds(i * 128, 128)], in_sem.at[1 + 2 * n + i])
-            )
-            copies[-1].start()
-        w_copies.append((pair, copies))
-    wq_copy = pltpu.make_async_copy(wq_hbm, wq, in_sem.at[9])
-    wq_copy.start()
-
     barrier = pltpu.get_barrier_semaphore()
     for k in range(NZ):
         z = lax.rem(me_z + k, NZ)
@@ -77,14 +57,29 @@
     for peer in (up, down):
         pl.semaphore_signal(barrier, inc=1, device_id={"kv": peer}, device_id_type=MESH)
 
+    x_copy = pltpu.make_async_copy(x_hbm, x, in_sem.at[0])
+    x_copy.start()
+    w_copies = []
+    parity = lax.rem(me_z, 2)
+    for n, turn in enumerate((0, 3 - 2 * parity, 1 + 2 * parity, 2)):
+        pair = lax.rem(me_z // 2 + turn, NZ // 2)
+        cols = pl.ds(pl.multiple_of(pair * 128, 128), 128)
+        copies = []
+        for i, src in enumerate((wk_hbm, wv_hbm)):
+            copies.append(
+                pltpu.make_async_copy(src.at[:, cols], wkv.at[n, :, pl.ds(i * 128, 128)], in_sem.at[1 + 2 * n + i])
+            )
+            if n == 0:
+                copies[-1].start()
+        w_copies.append((pair, copies))
+    wq_copy = pltpu.make_async_copy(wq_hbm, wq, in_sem.at[9])
+
     cs[...] = jnp.zeros_like(cs)
     cs[:, 0:PICKS] = jnp.maximum(chosen_ref[...], 0)
     lane = lax.broadcasted_iota(jnp.int32, (rows, 128), 1)
     low = lane < HEAD_DIM
 
     far = lax.rem(me_z + NZ // 2, NZ)
-    left = lax.rem(me_z + NZ - 1, NZ)
-    right = lax.rem(me_z + 1, NZ)
 
     def kv_copy(z):
         return pltpu.make_async_remote_copy(
@@ -108,30 +103,6 @@
         return pltpu.make_async_remote_copy(
             src_ref=cs, dst_ref=cland.at[src], send_sem=c_send.at[z],
             recv_sem=c_recv.at[src], device_id={"kv": at(z)}, device_id_type=MESH,
-        )
-
-    def kv_first_leg():
-        return pltpu.make_async_remote_copy(
-            src_ref=kvs.at[far], dst_ref=relay_kv, send_sem=kv_send.at[far],
-            recv_sem=relay_recv.at[0], device_id={"kv": at(left)}, device_id_type=MESH,
-        )
-
-    def kv_second_leg():
-        return pltpu.make_async_remote_copy(
-            src_ref=relay_kv, dst_ref=land.at[pl.ds(at(right) * blocks, blocks)], send_sem=relay_send.at[0],
-            recv_sem=kv_recv.at[right], device_id={"kv": at(lax.rem(right + NZ // 2, NZ))}, device_id_type=MESH,
-        )
-
-    def q_first_leg():
-        return pltpu.make_async_remote_copy(
-            src_ref=qs.at[far], dst_ref=relay_q, send_sem=q_send.at[far],
-            recv_sem=relay_recv.at[1], device_id={"kv": at(left)}, device_id_type=MESH,
-        )
-
-    def q_second_leg():
-        return pltpu.make_async_remote_copy(
-            src_ref=relay_q, dst_ref=qland.at[right], send_sem=relay_send.at[1],
-            recv_sem=q_recv.at[right], device_id={"kv": at(lax.rem(right + NZ // 2, NZ))}, device_id_type=MESH,
         )
 
     def y_copy(z, way, src=None):
@@ -144,7 +115,10 @@
     own_kv = pltpu.make_async_copy(kvs.at[me_z], land.at[pl.ds(kv * blocks, blocks)], own_sem.at[0])
     own_c = pltpu.make_async_copy(cs, cland.at[me_z], own_sem.at[1])
     x_copy.wait()
-    parity = lax.rem(me_z, 2)
+    for _, copies in w_copies[1:]:
+        for c in copies:
+            c.start()
+    wq_copy.start()
     for n, (pair, copies) in enumerate(w_copies):
         for c in copies:
             c.wait()
@@ -162,17 +136,11 @@
             own_kv.start()
             kv_copy(2 * pair + 1 - parity).start()
         elif n < 3:
-            for m in ((0, 1) if n == 1 else (1, 0)):
-                kv_copy(2 * pair + m).start()
+            near = 1 - parity if n == 1 else parity
+            kv_copy(2 * pair + near).start()
+            kv_copy(2 * pair + 1 - near).start()
         else:
-            @pl.when(core == 0)
-            def _():
-                kv_copy(far).start()
-
-            @pl.when(core == 1)
-            def _():
-                kv_first_leg().start()
-
+            kv_copy(far).start()
             kv_copy(2 * pair + 1 - parity).start()
 
     wo_rows = wo_hbm.shape[0]
@@ -185,31 +153,26 @@
     )
     wo_remote.start()
 
-    wq_copy.wait()
-
-    def project_queries(i, carry):
-        res = jnp.dot(x[...], wq[:, pl.ds(pl.multiple_of(i * 256, 256), 256)], preferred_element_type=F32)
-        lo = low[:half]
-        for u in range(2):
-            top, bot = res[:half, u * 128:(u + 1) * 128], res[half:, u * 128:(u + 1) * 128]
-            qs[4 * i + 2 * u] = jnp.where(lo, top, pltpu.roll(bot, HEAD_DIM, 1)).astype(BF16)
-            qs[4 * i + 2 * u + 1] = jnp.where(lo, pltpu.roll(top, HEAD_DIM, 1), bot).astype(BF16)
-        return carry
-
-    lax.fori_loop(0, 2, project_queries, 0)
     own_q = pltpu.make_async_copy(qs.at[me_z], qland.at[me_z], own_sem.at[2])
-    own_q.start()
-
-    @pl.when(core == 0)
-    def _():
-        q_copy(far, me_z).start()
-
-    @pl.when(core == 1)
-    def _():
-        q_first_leg().start()
-
-    for t in range(6, 0, -1):
-        q_copy(arrival_order(t, me_z), me_z).start()
+
+    def project_all_queries():
+        wq_copy.wait()
+
+        def project_queries(i, carry):
+            res = jnp.dot(x[...], wq[:, pl.ds(pl.multiple_of(i * 256, 256), 256)], preferred_element_type=F32)
+            lo = low[:half]
+            for u in range(2):
+                top, bot = res[:half, u * 128:(u + 1) * 128], res[half:, u * 128:(u + 1) * 128]
+                qs[4 * i + 2 * u] = jnp.where(lo, top, pltpu.roll(bot, HEAD_DIM, 1)).astype(BF16)
+                qs[4 * i + 2 * u + 1] = jnp.where(lo, pltpu.roll(top, HEAD_DIM, 1), bot).astype(BF16)
+            return carry
+
+        lax.fori_loop(0, 2, project_queries, 0)
+
+    def send_queries():
+        own_q.start()
+        for t in range(7, 0, -1):
+            q_copy(arrival_order(t, me_z), me_z).start()
 
     def y_arrival(z, way):
         rng = pl.ds((z * NY + (below, above)[way]) * blocks, blocks)
@@ -235,26 +198,20 @@
         )
 
     own_kv.wait()
-    for t in range(1, NZ + 1):
-        if t < NZ:
-            z = arrival_order(t, me_z)
+    for from_z, t in ((1, 1), (1, 2), (0, 0), (0, 1), (1, 3), (1, 4), (0, 2), (0, 3), (1, 5), (1, 6), (0, 4), (1, 7), (0, 5), (0, 6), (0, 7)):
+        z = arrival_order(t, me_z)
+        if from_z:
             kv_arrival(z).wait_recv()
             for way in range(2):
                 y_copy(z, way).start()
-        z = arrival_order(t - 1, me_z)
-        for way in range(2):
-            y_arrival(z, way).wait_recv()
-            f_copy(z, way).start()
-        if t == 5:
-            @pl.when(core == 1)
-            def _():
-                kv_first_leg().wait_recv()
-                kv_second_leg().start()
-        if t == 6:
-            @pl.when(core == 1)
-            def _():
-                q_first_leg().wait_recv()
-                q_second_leg().start()
+        else:
+            for way in range(2):
+                y_arrival(z, way).wait_recv()
+                f_copy(z, way).start()
+        if (from_z, t) == (0, 1):
+            project_all_queries()
+        if (from_z, t) == (1, 7):
+            send_queries()
     for z in range(NZ):
         for way in range(2):
             f_arrival(z, way).wait_recv()
@@ -413,11 +370,6 @@
         l_copy(z, me_z).wait_send()
     o_copy(me_z, 1 - core).wait_send()
 
-    @pl.when(core == 1)
-    def _():
-        kv_second_leg().wait_send()
-        q_second_leg().wait_send()
-
     for z in range(NZ):
         for way in range(2):
             y_copy(z, way).wait_send()
@@ -450,8 +402,6 @@
             pltpu.VMEM((8, 128), jnp.int32),
             pltpu.VMEM((NZ, 8, 128), jnp.int32),
             pltpu.SMEM((NZ, 8, 128), jnp.int32),
-            pltpu.VMEM((rows // BLOCK, BLOCK, 128), BF16),
-            pltpu.VMEM((rows // 2, 128), BF16),
             pltpu.VMEM((2, 2, BLOCK, PICKS * BLOCK), F32),
             pltpu.VMEM((NZ, 2, 128, 128), BF16),
             pltpu.VMEM((2 * NZ, 128, 128), BF16),
@@ -461,10 +411,10 @@
             pltpu.VMEM((rows // 2, 2 * width), BF16),
             dma((10,)), dma, dma, dma, dma((3,)), dma((2,)), dma,
             dma((NZ,)), dma((NZ,)), dma((NZ,)), dma((NZ,)), dma((NZ,)), dma((NZ,)),
-            dma((2,)), dma((2,)), dma((NZ, 2)), dma((NZ, 2)), dma((NZ, 2)), dma((NZ, 2)),
+            dma((NZ, 2)), dma((NZ, 2)), dma((NZ, 2)), dma((NZ, 2)),
             dma((NZ, 2)), dma((2 * NZ,)), dma((NZ,)), dma((NZ,)),
         ],
-        compiler_params=pltpu.CompilerParams(collective_id=0, has_side_effects=True, vmem_limit_bytes=62 * 2**20),
+        compiler_params=pltpu.CompilerParams(collective_id=0, has_side_effects=True, vmem_limit_bytes=52 * 2**20),
         name="heads_over_z",
     )(tokens[0], w_query, w_key, w_value, w_out, chosen[0])
     return mixed[None], log_sums[None]

time: 81.3 us -> 72.9 us (0.90)
  Pallas kernels: 77.6 us -> 69.9 us
    pallas_call x1, Pallas kernels: 77.6 us -> 69.9 us  [on_device(): pl.pallas_call(kernel, out_shape=(jax.ShapeDtypeStruct((rows // 2, model)...]
where the time goes in v3:
time: 72.9 us; the launch traced here: 72.8 us
  Pallas kernels  69.9 us (96%)
  local copies, waits for them, and re-layouts  2.26 us (3%)
    pallas_call x1, Pallas kernels, on_device(): pl.pallas_call(kernel, out_shape=(jax.ShapeDtypeStruct((rows // 2, model)...  69.9 us
    unnamed x4, local copies, waits for them, and re-layouts  2.26 us

profile of v3, /device:TPU:1, one launch (start us, length us, event | category | flops | bytes accessed | tf_op | source)
XLA Modules:
  0.0 72.8 jit_solution(14628885984656118896)
XLA Ops:
  0.6 0.0 copy-start
  0.6 0.7 copy-done
  1.3 69.9 %heads_over_z.1 = (bf16[256,2048]{1,0:T(8,128)(2,1)S(1)}, f32[8,512]{1,0:T(8,128)S(1)}) custom-call(bf16[512,2048]{1,0:T(8,128)(2,1)} %bitcast.7, bf16[2048,512]{1,0:T(8,128)(2,1)} %wq_hbm.1, bf16[2048,512]{1,0:T(8,128)(2,1)} %wk_hbm.1, bf16[2048,512]{1,0:T(8,128)(2,1)} %wv_hbm.1, bf16[512,2048]{1,0:T(8,128)(2,1)} %wo_hbm.1, s32[8,16]{1,0:T(8,128)S(1)} %bitcast.6), custom_call_target="tpu_custom_call" | custom-call | tf_op jit(solution)/shard_map/heads_over_z/pallas_call | solution.py:385
  71.2 1.0 %copy.10 = bf16[1,256,2048]{2,1,0:T(8,128)(2,1)} copy(bf16[1,256,2048]{2,1,0:T(8,128)(2,1)S(1)} %bitcast.4) | data formatting | bytes 2097152
  72.2 0.6 copy.11
Async XLA Ops:
  0.6 0.7 copy-start

commit v4 on v3

--- a/solution.py
+++ b/solution.py
@@ -11,7 +11,11 @@
 BLOCK = 64
 NZ = 8
 NY = 4
+EVENTS = (
+    (1, 1), (1, 2), (0, 0), (0, 1), (1, 3), (1, 4), (0, 2), (0, 3), (1, 5), (0, 4), (1, 6), (1, 7), (0, 5), (0, 6),
+)
 PICKS = 16
+EARLY = 3
 LOG2E = 1.4426950408889634
 MESH = pl.DeviceIdType.MESH
 BF16 = jnp.bfloat16
@@ -25,9 +29,38 @@
     return lax.rem(me_z + offset, NZ)
 
 
+def gather_table():
+    table = []
+    for z in range(NZ):
+        sign = 1 if z % 2 == 0 else -1
+        offsets = [0, sign, -sign, 2 * sign, -2 * sign, 3 * sign, -3 * sign, 4]
+        last = {4: 7, 5: 7, 6: 3}.get(z, (z + 4) % NZ)
+        found = [(z + o) % NZ for o in offsets]
+        found.remove(last)
+        table.append(found + [last])
+    return table
+
+
+def group_table():
+    table = []
+    for z in range(NZ):
+        last = gather_table()[z][-1]
+        far_first = sorted((g for g in range(NZ) if g != z), key=lambda g: -min((g - z) % NZ, (z - g) % NZ))
+        early = [g for g in far_first if g < last][:EARLY]
+        table.append(early + [g for g in far_first if g not in early] + [z])
+    return table
+
+
+def lookup(table, step, me_z):
+    value = table[0][step]
+    for z in range(1, NZ):
+        value = jnp.where(me_z == z, table[z][step], value)
+    return value
+
+
 def kernel(
-    x_hbm, wq_hbm, wk_hbm, wv_hbm, wo_hbm, chosen_ref, out_ref, logs_ref,
-    x, wkv, wq, wo, kvs, land, qs, qland, cs, cland, picks, scores, os, oland, stat, ls, lland, att,
+    x_hbm, wq_hbm, wk_hbm, wv_hbm, wo_hbm, chosen_hbm, out_ref, logs_ref,
+    x, wkv, wq, wo, kvs, land, late, listing, qs, qland, cs, cland, picks, scores, os, oland, stat, ls, lland, att,
     in_sem, wo_sem, wo_send, wo_recv, own_sem, own_out_sem, pick_sem,
     kv_send, kv_recv, q_send, q_recv, c_send, c_recv,
     y_send, y_recv, f_send, f_recv, o_send, o_recv, l_send, l_recv,
@@ -46,6 +79,10 @@
     def at(z):
         return z * NY + me_y
 
+    gather_order = [lookup(gather_table(), t, me_z) for t in range(NZ)]
+    group_order = [lookup(group_table(), t, me_z) for t in range(NZ)]
+    last_z = gather_order[-1]
+
     barrier = pltpu.get_barrier_semaphore()
     for k in range(NZ):
         z = lax.rem(me_z + k, NZ)
@@ -59,6 +96,8 @@
 
     x_copy = pltpu.make_async_copy(x_hbm, x, in_sem.at[0])
     x_copy.start()
+    list_copy = pltpu.make_async_copy(chosen_hbm, listing, pick_sem)
+    list_copy.start()
     w_copies = []
     parity = lax.rem(me_z, 2)
     for n, turn in enumerate((0, 3 - 2 * parity, 1 + 2 * parity, 2)):
@@ -75,7 +114,8 @@
     wq_copy = pltpu.make_async_copy(wq_hbm, wq, in_sem.at[9])
 
     cs[...] = jnp.zeros_like(cs)
-    cs[:, 0:PICKS] = jnp.maximum(chosen_ref[...], 0)
+    list_copy.wait()
+    cs[:, 0:PICKS] = jnp.maximum(listing[...], 0)
     lane = lax.broadcasted_iota(jnp.int32, (rows, 128), 1)
     low = lane < HEAD_DIM
 
@@ -146,12 +186,10 @@
     wo_rows = wo_hbm.shape[0]
     wo_mine = wo.at[pl.ds(core * wo_rows, wo_rows)]
     wo_local = pltpu.make_async_copy(wo_hbm, wo_mine, wo_sem)
-    wo_local.start()
     wo_remote = pltpu.make_async_remote_copy(
         src_ref=wo_hbm, dst_ref=wo_mine, send_sem=wo_send, recv_sem=wo_recv,
         device_id={"tp": 1 - core}, device_id_type=MESH,
     )
-    wo_remote.start()
 
     own_q = pltpu.make_async_copy(qs.at[me_z], qland.at[me_z], own_sem.at[2])
 
@@ -174,55 +212,68 @@
         for t in range(7, 0, -1):
             q_copy(arrival_order(t, me_z), me_z).start()
 
-    def y_arrival(z, way):
-        rng = pl.ds((z * NY + (below, above)[way]) * blocks, blocks)
-        return pltpu.make_async_remote_copy(
-            src_ref=land.at[rng], dst_ref=land.at[rng], send_sem=y_send.at[z, way],
-            recv_sem=y_recv.at[z, way], device_id={"kv": (up, down)[way]}, device_id_type=MESH,
-        )
-
-    def f_copy(z, way):
-        rng = pl.ds((z * NY + (below, above)[way]) * blocks + way * (blocks // 2), blocks // 2)
-        return pltpu.make_async_remote_copy(
-            src_ref=land.at[rng], dst_ref=land.at[rng], send_sem=f_send.at[z, way],
-            recv_sem=f_recv.at[z, way], device_id={"kv": (up, down)[way]}, device_id_type=MESH,
+    def late_copy(way):
+        rng = pl.ds(me_y * blocks, blocks)
+        return pltpu.make_async_remote_copy(
+            src_ref=land.at[pl.ds(at(last_z) * blocks, blocks)], dst_ref=late.at[rng], send_sem=y_send.at[last_z, way],
+            recv_sem=y_recv.at[last_z, way], device_id={"kv": (up, down)[way]}, device_id_type=MESH,
+        )
+
+    def arrived(buffer, first, count, sems, z, way):
+        rng = pl.ds(first, count)
+        return pltpu.make_async_remote_copy(
+            src_ref=buffer.at[rng], dst_ref=buffer.at[rng], send_sem=sems[0].at[z, way],
+            recv_sem=sems[1].at[z, way], device_id={"kv": (up, down)[way]}, device_id_type=MESH,
         )
 
     across = lax.rem(me_y + 2, NY)
 
-    def f_arrival(z, way):
-        rng = pl.ds((z * NY + across) * blocks + way * (blocks // 2), blocks // 2)
-        return pltpu.make_async_remote_copy(
-            src_ref=land.at[rng], dst_ref=land.at[rng], send_sem=f_send.at[z, way],
-            recv_sem=f_recv.at[z, way], device_id={"kv": (up, down)[way]}, device_id_type=MESH,
-        )
-
+    def base(z, late_one):
+        return 0 if late_one else z * NY * blocks
+
+    def y_arrival(z, way, late_one=False):
+        first = base(z, late_one) + (below, above)[way] * blocks
+        return arrived(late if late_one else land, first, blocks, (y_send, y_recv), z, way)
+
+    def f_copy(z, way, late_one=False):
+        first = base(z, late_one) + (below, above)[way] * blocks + way * (blocks // 2)
+        return arrived(late if late_one else land, first, blocks // 2, (f_send, f_recv), z, way)
+
+    def f_arrival(z, way, late_one=False):
+        first = base(z, late_one) + across * blocks + way * (blocks // 2)
+        return arrived(late if late_one else land, first, blocks // 2, (f_send, f_recv), z, way)
+
+    to_scalars = pltpu.make_async_copy(cland, picks, pick_sem)
     own_kv.wait()
-    for from_z, t in ((1, 1), (1, 2), (0, 0), (0, 1), (1, 3), (1, 4), (0, 2), (0, 3), (1, 5), (1, 6), (0, 4), (1, 7), (0, 5), (0, 6), (0, 7)):
-        z = arrival_order(t, me_z)
+    for from_z, t in EVENTS:
+        z = gather_order[t]
         if from_z:
             kv_arrival(z).wait_recv()
             for way in range(2):
-                y_copy(z, way).start()
+                (y_copy(z, way) if t < NZ - 1 else late_copy(way)).start()
         else:
             for way in range(2):
                 y_arrival(z, way).wait_recv()
                 f_copy(z, way).start()
         if (from_z, t) == (0, 1):
             project_all_queries()
-        if (from_z, t) == (1, 7):
+            stat[...] = jnp.zeros_like(stat)
+        if (from_z, t) == (0, 4):
+            wo_local.start()
+            wo_remote.start()
+        if (from_z, t) == (0, 3):
+            own_c.wait()
+            for k in range(1, NZ):
+                src = arrival_order(k, me_z)
+                c_copy(src, src).wait_recv()
+            to_scalars.start()
+        if (from_z, t) == (1, NZ - 2):
             send_queries()
-    for z in range(NZ):
+    for t in range(NZ - 1):
         for way in range(2):
-            f_arrival(z, way).wait_recv()
-
-    own_c.wait()
+            f_arrival(gather_order[t], way).wait_recv()
+
     own_q.wait()
-    for t in range(1, NZ):
-        z = arrival_order(t, me_z)
-        c_copy(z, z).wait_recv()
-    to_scalars = pltpu.make_async_copy(cland, picks, pick_sem)
-    to_scalars.start()
     to_scalars.wait()
 
     lane_iota = lax.broadcasted_iota(jnp.int32, (128, 128), 1)
@@ -265,6 +316,7 @@
 
     def finish(g, j, slot):
         device = g * NY + me_y
+        exps, totals = [], []
         for i in range(2):
             bias = jnp.where(key_row < (j + 4 * i + 2 * device + 1) * BLOCK, 0.0, -jnp.inf)
             s = scores[slot, i] + bias
@@ -272,21 +324,32 @@
             peak = jnp.max(s, axis=1, keepdims=True)
             e = jnp.exp2((s - peak) * (LOG2E * HEAD_DIM ** -0.5))
             total = jnp.sum(e, axis=1, keepdims=True)
-            part = jnp.dot(e.astype(BF16), listed(g, j + 4 * i), preferred_element_type=F32) * (1.0 / total)
             log_sum = peak * HEAD_DIM ** -0.5 + jnp.log(total)
             band = slice(i * BLOCK, (i + 1) * BLOCK)
             stat[band, :] = jnp.where(lane_iota[band] == j, log_sum, stat[band, :])
+            exps.append(e.astype(BF16))
+            totals.append(total)
+        values = jnp.concatenate([listed(g, j), listed(g, j + 4)], axis=1)
+        both = jnp.dot(jnp.concatenate(exps, axis=0), values, preferred_element_type=F32)
+        for i in range(2):
+            part = both[i * BLOCK:(i + 1) * BLOCK, i * 128:(i + 1) * 128] * (1.0 / totals[i])
             place = slice((j % 2) * BLOCK, (j % 2 + 1) * BLOCK)
             if j < 2:
                 os[g, i, place, :] = pltpu.roll(part, HEAD_DIM, 1).astype(BF16)
             else:
                 os[g, i, place, :] = jnp.where(low64, os[g, i, place, :].astype(F32), part).astype(BF16)
 
+    def group(t):
+        value = group_order[0]
+        for k in range(1, NZ):
+            value = jnp.where(t == k, group_order[k], value)
+        return value
+
     def attend_group(t, carry):
-        g = arrival_order(NZ - 1 - t, me_z)
-        following = arrival_order(jnp.maximum(NZ - 2 - t, 0), me_z)
-
-        @pl.when(t < NZ - 2)
+        g = group(t)
+        following = group(jnp.where(t == EARLY - 1, t, jnp.minimum(t + 1, NZ - 1)))
+
+        @pl.when((t < NZ - 2) & (t != EARLY - 1))
         def _():
             q_copy(following, following).wait_recv()
 
@@ -296,7 +359,7 @@
             else:
                 score(following, 0, 0)
             finish(g, j, j % 2)
-        ls[g] = stat[...].T[0:8]
+        ls[g] = stat[...].T[0:4]
 
         @pl.when(g != me_z)
         def _():
@@ -312,11 +375,21 @@
 
         return carry
 
-    stat[...] = jnp.zeros_like(stat)
-    os[...] = jnp.zeros_like(os)
-    q_copy(far, far).wait_recv()
-    score(far, 0, 0)
-    lax.fori_loop(0, NZ, attend_group, 0)
+    q_copy(group_order[0], group_order[0]).wait_recv()
+    score(group_order[0], 0, 0)
+    lax.fori_loop(0, 1, attend_group, 0)
+    for way in range(2):
+        y_arrival(last_z, way, True).wait_recv()
+        f_copy(last_z, way, True).start()
+    lax.fori_loop(1, EARLY, attend_group, 0)
+    for way in range(2):
+        f_arrival(last_z, way, True).wait_recv()
+    for k in range(1, NY):
+        y = lax.rem(me_y + k, NY)
+        land[pl.ds((last_z * NY + y) * blocks, blocks)] = late[pl.ds(y * blocks, blocks)]
+    q_copy(group_order[EARLY], group_order[EARLY]).wait_recv()
+    score(group_order[EARLY], 0, 0)
+    lax.fori_loop(EARLY, NZ, attend_group, 0)
 
     def o_arrival(head):
         return pltpu.make_async_remote_copy(
@@ -388,7 +461,7 @@
             jax.ShapeDtypeStruct((rows // 2, model), BF16),
             jax.ShapeDtypeStruct((width // HEAD_DIM, rows), F32),
         ),
-        in_specs=[hbm] * 5 + [vmem],
+        in_specs=[hbm] * 6,
         out_specs=(vmem, vmem),
         scratch_shapes=[
             pltpu.VMEM((rows, model), BF16),
@@ -397,6 +470,8 @@
             pltpu.VMEM((2 * width, model), BF16),
             pltpu.VMEM((NZ, rows // BLOCK, BLOCK, 128), BF16),
             pltpu.VMEM((NZ * NY * rows // BLOCK, BLOCK, 128), BF16),
+            pltpu.VMEM((NY * rows // BLOCK, BLOCK, 128), BF16),
+            pltpu.VMEM(chosen.shape[1:], jnp.int32),
             pltpu.VMEM((NZ, rows // 2, 128), BF16),
             pltpu.VMEM((NZ, rows // 2, 128), BF16),
             pltpu.VMEM((8, 128), jnp.int32),
@@ -406,8 +481,8 @@
             pltpu.VMEM((NZ, 2, 128, 128), BF16),
             pltpu.VMEM((2 * NZ, 128, 128), BF16),
             pltpu.VMEM((128, 128), F32),
-            pltpu.VMEM((NZ, 8, 128), F32),
-            pltpu.VMEM((NZ, 8, 128), F32),
+            pltpu.VMEM((NZ, 4, 128), F32),
+            pltpu.VMEM((NZ, 4, 128), F32),
             pltpu.VMEM((rows // 2, 2 * width), BF16),
             dma((10,)), dma, dma, dma, dma((3,)), dma((2,)), dma,
             dma((NZ,)), dma((NZ,)), dma((NZ,)), dma((NZ,)), dma((NZ,)), dma((NZ,)),

time: 72.9 us -> 70.7 us (0.970)
  Pallas kernels: 69.9 us -> 67.7 us
    pallas_call x1, Pallas kernels: 69.9 us -> 67.7 us  [on_device(): pl.pallas_call(kernel, out_shape=(jax.ShapeDtypeStruct((rows // 2, model)...]
where the time goes in v4:
time: 70.7 us; the launch traced here: 70.6 us
  Pallas kernels  67.7 us (96%)
  local copies, waits for them, and re-layouts  2.26 us (3%)
    pallas_call x1, Pallas kernels, on_device(): pl.pallas_call(kernel, out_shape=(jax.ShapeDtypeStruct((rows // 2, model)...  67.7 us
    unnamed x4, local copies, waits for them, and re-layouts  2.26 us

profile of v4, /device:TPU:1, one launch (start us, length us, event | category | flops | bytes accessed | tf_op | source)
XLA Modules:
  0.0 70.6 jit_solution(17219192083405139229)
XLA Ops:
  0.6 0.0 copy-start
  0.6 0.7 copy-done
  1.3 67.7 %heads_over_z.1 = (bf16[256,2048]{1,0:T(8,128)(2,1)S(1)}, f32[8,512]{1,0:T(8,128)S(1)}) custom-call(bf16[512,2048]{1,0:T(8,128)(2,1)} %bitcast.7, bf16[2048,512]{1,0:T(8,128)(2,1)} %wq_hbm.1, bf16[2048,512]{1,0:T(8,128)(2,1)} %wk_hbm.1, bf16[2048,512]{1,0:T(8,128)(2,1)} %wv_hbm.1, bf16[512,2048]{1,0:T(8,128)(2,1)} %wo_hbm.1, s32[8,16]{1,0:T(8,128)S(1)} %bitcast.6), custom_call_target="tpu_custom_call" | custom-call | tf_op jit(solution)/shard_map/heads_over_z/pallas_call | solution.py:458
  69.0 1.0 %copy.10 = bf16[1,256,2048]{2,1,0:T(8,128)(2,1)} copy(bf16[1,256,2048]{2,1,0:T(8,128)(2,1)S(1)} %bitcast.4) | data formatting | bytes 2097152
  70.0 0.6 copy.11
Async XLA Ops:
  0.6 0.7 copy-start

commit v5 on v4

--- a/solution.py
+++ b/solution.py
@@ -12,7 +12,7 @@
 NZ = 8
 NY = 4
 EVENTS = (
-    (1, 1), (1, 2), (0, 0), (0, 1), (1, 3), (1, 4), (0, 2), (0, 3), (1, 5), (0, 4), (1, 6), (1, 7), (0, 5), (0, 6),
+    (1, 1), (1, 2), (0, 0), (0, 1), (1, 3), (1, 4), (0, 2), (0, 3), (1, 5), (1, 6), (0, 4), (1, 7), (0, 5), (0, 6),
 )
 PICKS = 16
 EARLY = 3

time: 70.7 us -> 69.6 us (0.984)
  Pallas kernels: 67.7 us -> 66.6 us
    pallas_call x1, Pallas kernels: 67.7 us -> 66.6 us  [on_device(): pl.pallas_call(kernel, out_shape=(jax.ShapeDtypeStruct((rows // 2, model)...]
where the time goes in v5:
time: 69.6 us; the launch traced here: 69.5 us
  Pallas kernels  66.6 us (96%)
  local copies, waits for them, and re-layouts  2.26 us (3%)
    pallas_call x1, Pallas kernels, on_device(): pl.pallas_call(kernel, out_shape=(jax.ShapeDtypeStruct((rows // 2, model)...  66.6 us
    unnamed x4, local copies, waits for them, and re-layouts  2.26 us

profile of v5, /device:TPU:1, one launch (start us, length us, event | category | flops | bytes accessed | tf_op | source)
XLA Modules:
  0.0 69.5 jit_solution(3641402715294281297)
XLA Ops:
  0.6 0.0 copy-start
  0.6 0.7 copy-done
  1.3 66.6 %heads_over_z.1 = (bf16[256,2048]{1,0:T(8,128)(2,1)S(1)}, f32[8,512]{1,0:T(8,128)S(1)}) custom-call(bf16[512,2048]{1,0:T(8,128)(2,1)} %bitcast.7, bf16[2048,512]{1,0:T(8,128)(2,1)} %wq_hbm.1, bf16[2048,512]{1,0:T(8,128)(2,1)} %wk_hbm.1, bf16[2048,512]{1,0:T(8,128)(2,1)} %wv_hbm.1, bf16[512,2048]{1,0:T(8,128)(2,1)} %wo_hbm.1, s32[8,16]{1,0:T(8,128)S(1)} %bitcast.6), custom_call_target="tpu_custom_call" | custom-call | tf_op jit(solution)/shard_map/heads_over_z/pallas_call | solution.py:458
  67.9 1.0 %copy.10 = bf16[1,256,2048]{2,1,0:T(8,128)(2,1)} copy(bf16[1,256,2048]{2,1,0:T(8,128)(2,1)S(1)} %bitcast.4) | data formatting | bytes 2097152
  68.9 0.6 copy.11
Async XLA Ops:
  0.6 0.7 copy-start

commit v6 on v5

--- a/solution.py
+++ b/solution.py
@@ -399,18 +399,24 @@
 
     pltpu.make_async_copy(os.at[me_z, core], oland.at[core * NZ + me_z], own_out_sem.at[0]).wait()
     pltpu.make_async_copy(ls.at[me_z], lland.at[me_z], own_out_sem.at[1]).wait()
+    low128 = lane_iota < HEAD_DIM
+    for turn in (2, 1, 3, 0):
+        pair = lax.rem(me_z // 2 + turn, NZ // 2)
+        for c in range(2):
+            for m in range(2):
+                z = 2 * pair + m
+
+                @pl.when((z != me_z) | (core != c))
+                def _():
+                    o_arrival(c * NZ + z).wait_recv()
+
+            a, b = oland[c * NZ + 2 * pair].astype(F32), oland[c * NZ + 2 * pair + 1].astype(F32)
+            cols = pl.ds(pl.multiple_of((c * NZ // 2 + pair) * 128, 128), 128)
+            att[0:128, cols] = jnp.where(low128, a, pltpu.roll(b, HEAD_DIM, 1)).astype(BF16)
+            att[128:256, cols] = jnp.where(low128, pltpu.roll(a, HEAD_DIM, 1), b).astype(BF16)
     for t in range(1, NZ):
         z = arrival_order(t, me_z)
-        o_arrival(core * NZ + z).wait_recv()
         l_copy(z, z).wait_recv()
-    for z in range(NZ):
-        o_arrival((1 - core) * NZ + z).wait_recv()
-    low128 = lane_iota < HEAD_DIM
-    for i in range(NZ):
-        a, b = oland[2 * i].astype(F32), oland[2 * i + 1].astype(F32)
-        cols = pl.ds(i * 128, 128)
-        att[0:128, cols] = jnp.where(low128, a, pltpu.roll(b, HEAD_DIM, 1)).astype(BF16)
-        att[128:256, cols] = jnp.where(low128, pltpu.roll(a, HEAD_DIM, 1), b).astype(BF16)
     low8 = low128[:8]
     for h in range(NZ):
         mine = lland[h]

time: 69.6 us -> 69.6 us (level)
  no operation moved by 1% of the time
where the time goes in v6:
time: 69.6 us; the launch traced here: 69.5 us
  Pallas kernels  66.6 us (96%)
  local copies, waits for them, and re-layouts  2.26 us (3%)
    pallas_call x1, Pallas kernels, on_device(): pl.pallas_call(kernel, out_shape=(jax.ShapeDtypeStruct((rows // 2, model)...  66.6 us
    unnamed x4, local copies, waits for them, and re-layouts  2.26 us

profile of v6, /device:TPU:1, one launch (start us, length us, event | category | flops | bytes accessed | tf_op | source)
XLA Modules:
  0.0 69.5 jit_solution(12227891924759748811)
XLA Ops:
  0.6 0.0 copy-start
  0.6 0.7 copy-done
  1.3 66.6 %heads_over_z.1 = (bf16[256,2048]{1,0:T(8,128)(2,1)S(1)}, f32[8,512]{1,0:T(8,128)S(1)}) custom-call(bf16[512,2048]{1,0:T(8,128)(2,1)} %bitcast.7, bf16[2048,512]{1,0:T(8,128)(2,1)} %wq_hbm.1, bf16[2048,512]{1,0:T(8,128)(2,1)} %wk_hbm.1, bf16[2048,512]{1,0:T(8,128)(2,1)} %wv_hbm.1, bf16[512,2048]{1,0:T(8,128)(2,1)} %wo_hbm.1, s32[8,16]{1,0:T(8,128)S(1)} %bitcast.6), custom_call_target="tpu_custom_call" | custom-call | tf_op jit(solution)/shard_map/heads_over_z/pallas_call | solution.py:464
  67.9 1.0 %copy.10 = bf16[1,256,2048]{2,1,0:T(8,128)(2,1)} copy(bf16[1,256,2048]{2,1,0:T(8,128)(2,1)S(1)} %bitcast.4) | data formatting | bytes 2097152
  68.9 0.6 copy.11
Async XLA Ops:
  0.6 0.7 copy-start
